TPU v7x, 512 devices: a whole 4x8x8 slice. The times are simulated.
512 devices in a mesh: ep: 32 (over z, x), tp: 16 (over y, core).
Axes of the slice: x: 4, y: 8, z: 8, core: 2. Of those that a mesh axis runs over, the one named last changes fastest.
Arguments:
- receptance: bfloat16 [16384, 1024], P('ep', 'tp'), may hold values from -6 to 6
- key_matrix: bfloat16 [16384, 1024], P('ep', 'tp'), may hold values from -6 to 6
- value_matrix: bfloat16 [16384, 1024], P('ep', 'tp'), may hold values from -6 to 6
- decay_data_term: bfloat16 [16384, 1024], P('ep', 'tp'), may hold values from -3.5 to 3.5
- correction_rate_data: bfloat16 [16384, 1024], P('ep', 'tp'), may hold values from -6 to 6
- output_gate_input: bfloat16 [16384, 1024], P('ep', 'tp'), may hold values from -6 to 6
- decay_channel_offset: float32 [1024], P('tp'), may hold values from -12 to -2
- correction_rate_offset: float32 [1024], P('tp'), may hold values from -12 to 1
- extra_head_log_decay: float32 [16384, 16], P('ep', 'tp'), may hold values from -2.1 to 0, as said below
- head_norm_gain: float32 [1024], P('tp'), may hold values from 0.1 to 1.9
- mixer_output_weight: bfloat16 [1024, 2048], P('tp'), may hold values from -0.1875 to 0.1875
- expert_layer_input: bfloat16 [4096, 2048], P('ep'), may hold values from -6 to 6
- feedforward_norm_gain: float32 [2048], replicated, may hold values from 0.1 to 1.9
- group_router_weight: bfloat16 [2048, 4], replicated, may hold values from -0.125 to 0.125
- expert_router_weight: bfloat16 [2048, 32], replicated, may hold values from -0.125 to 0.125
- routes: int32 [4096, 2], P('ep'), may hold values from 0 to 31, all different within a row; in each aligned block of 128 rows (0 to 127, 128 to 255, ...) at most 16 rows name the same one
- expert_gate_weight: bfloat16 [32, 2048, 4096], P('ep', None, 'tp'), may hold values from -0.125 to 0.125
- expert_up_weight: bfloat16 [32, 2048, 4096], P('ep', None, 'tp'), may hold values from -0.125 to 0.125
- expert_down_weight: bfloat16 [32, 4096, 2048], P('ep', 'tp'), may hold values from -0.09375 to 0.09375
Outputs:
- token_mixer_output: bfloat16 [16384, 2048], P(('ep', 'tp'))
- expert_out: bfloat16 [4096, 2048], P('ep', 'tp')
Inputs may be any that keep to these rules, and one draw needn't show every extreme that they name: A token's routes are distinct. Within the rows of one index of ep, no expert is named by more than 16 rows, a bound that some block reaches. `extra_head_log_decay`: entries are zero or negative; each head has a few nonzero positions.
All inputs are finite; a program needn't handle non-finite values.
Results may differ from a plain program's by a relative error of at most 0.022.
Values may be sent and summed in bfloat16 or wider, within the bound.
A program may use at most 64 MiB of HBM per device.

v0:
```python
import jax
import jax.numpy as jnp
from jax import lax
from jax.sharding import PartitionSpec as P

HEAD_DIM = 64
GROUPS = 4


key_eps = 1e-06
group_eps = 0.00064
norm_eps = 1e-06


def sent_to_all(value, axis):
    devices = lax.axis_size(axis)
    return lax.all_to_all(
        jnp.broadcast_to(value[None], (devices, *value.shape)), axis, 0, 0, tiled=True
    )


def all_in_one(value, axis):
    leaves = jax.tree.leaves(value)
    sequence = sorted(range(len(leaves)), key=lambda k: -leaves[k].size)
    width = (1, *leaves[sequence[0]].shape)[-1]
    lines = [
        jnp.pad(leaves[k].reshape(-1), (0, -leaves[k].size % width)).reshape(-1, width)
        for k in sequence
    ]
    both, at, found = (sent_to_all(jnp.concatenate(lines), axis), 0, {})
    for k, line in zip(sequence, lines):
        piece = both[:, at : at + len(line)].reshape(len(both), -1)
        found[k] = piece[:, : leaves[k].size].reshape(-1, *leaves[k].shape)
        at += len(line)
    numbers = iter(range(len(leaves)))
    return jax.tree.map(lambda _: found[next(numbers)], value)


def folded_in_pairs(pieces, combine):
    while len(jax.tree.leaves(pieces)[0]) > 1:
        pieces = jax.vmap(combine)(
            *(jax.tree.map(lambda part: part[side::2], pieces) for side in (0, 1))
        )
    return jax.tree.map(lambda part: part[0], pieces)


def entering(value, axis, combine, identity):
    devices, place = (lax.axis_size(axis), lax.axis_index(axis))
    passed = jnp.arange(devices) < place

    def kept(part, zero, own):
        part = jnp.where(
            passed.reshape(-1, *(1 for _ in own.shape)),
            part.astype(own.dtype),
            jnp.asarray(zero, own.dtype),
        )
        return part

    pieces = all_in_one(
        jax.tree.map(lambda part, kind: part.astype(kind), value, (jnp.bfloat16, jnp.bfloat16)),
        axis,
    )
    return folded_in_pairs(jax.tree.map(kept, pieces, identity, value), combine)


def in_blocks(value, dim, devices):
    before, after = (value.shape[:dim], value.shape[dim + 1 :])
    return jnp.moveaxis(value.reshape(*before, devices, -1, *after), dim, 0)


def summed_on_arrival(value, axis, dim):
    parts = in_blocks(value, dim, lax.axis_size(axis))
    arrived = lax.all_to_all(parts, axis, split_axis=0, concat_axis=0, tiled=True)
    return arrived.astype(jnp.float32).sum(axis=0)


def chain_join(earlier, later):
    joined_map = jnp.einsum("hvk,hkj->hvj", earlier[0], later[0])
    joined_state = jnp.einsum("hvk,hkj->hvj", earlier[1], later[0]) + later[1]
    return (joined_map, joined_state)


def pair_decay(upper, lower, keep):
    gap = upper[:, None] - lower[None, :]
    mask = keep[:, :, None, None]
    return jnp.where(mask, jnp.exp(jnp.where(mask, gap, 0.0)), 0.0)


def block_advance(stacked, inputs):
    recept_b, log_b, unit_b, removal_b, key_b, value_b = inputs
    block_len = recept_b.shape[0]
    cumul = jnp.cumsum(log_b, axis=0)
    before = cumul - log_b
    places = jnp.arange(block_len)
    strict = places[:, None] > places[None, :]
    upto = places[:, None] >= places[None, :]
    strict_decay = pair_decay(before, cumul, strict)
    upto_decay = pair_decay(cumul, cumul, upto)
    key_pairs = jnp.einsum("jhk,ihk,jihk->hji", unit_b, key_b, strict_decay)
    removal_pairs = jnp.einsum("jhk,ihk,jihk->hji", unit_b, removal_b, strict_decay)
    read_keys = jnp.einsum("thk,ihk,tihk->hti", recept_b, key_b, upto_decay)
    read_removal = jnp.einsum("thk,ihk,tihk->hti", recept_b, removal_b, upto_decay)
    value_padded = jnp.concatenate([value_b, jnp.zeros_like(value_b)], axis=-1)
    right_side = jnp.einsum("jhk,hrk->hjr", unit_b * jnp.exp(before), stacked) + jnp.einsum(
        "hji,ihr->hjr", key_pairs, value_padded
    )
    left_side = jnp.eye(block_len, dtype=jnp.float32)[None] + removal_pairs
    corrected = jax.scipy.linalg.solve_triangular(
        left_side, right_side, lower=True, unit_diagonal=True
    )
    outputs = (
        jnp.einsum("thk,hrk->thr", recept_b * jnp.exp(cumul), stacked)
        + jnp.einsum("hti,ihr->thr", read_keys, value_padded)
        - jnp.einsum("hti,hir->thr", read_removal, corrected)
    )
    tail = jnp.exp(cumul[-1][None] - cumul)
    stacked = (
        stacked * jnp.exp(cumul[-1])[:, None, :]
        + jnp.einsum("ihr,ihk->hrk", value_padded, key_b * tail)
        - jnp.einsum("hir,ihk->hrk", corrected, removal_b * tail)
    )
    return (stacked, outputs)


def mixer_part(
    receptance,
    key_matrix,
    value_matrix,
    decay_data_term,
    correction_rate_data,
    output_gate_input,
    decay_channel_offset,
    correction_rate_offset,
    extra_head_log_decay,
    head_norm_gain,
    mixer_output_weight,
):
    positions = receptance.shape[0]
    head_count = receptance.shape[1] // HEAD_DIM

    def head_view(tensor_in):
        return tensor_in.astype(jnp.float32).reshape(positions, head_count, HEAD_DIM)

    recept = head_view(receptance)
    keyed = head_view(key_matrix)
    valued = head_view(value_matrix)
    unit_keys = keyed * lax.rsqrt(jnp.sum(keyed * keyed, axis=-1, keepdims=True) + key_eps)
    learn_rate = jax.nn.sigmoid(
        head_view(correction_rate_data) + correction_rate_offset.reshape(head_count, HEAD_DIM)
    )
    decay_preactivation = head_view(decay_data_term) + decay_channel_offset.reshape(
        head_count, HEAD_DIM
    )
    decay_logarithm = (
        -jnp.exp(-jax.nn.softplus(-decay_preactivation) - 0.5) + extra_head_log_decay[:, :, None]
    )
    removal = unit_keys * learn_rate
    block_len = min(64, positions)
    block_count = positions // block_len

    def blocked(tensor_in):
        return tensor_in.reshape(block_count, block_len, head_count, HEAD_DIM)

    eye_maps = jnp.broadcast_to(
        jnp.eye(HEAD_DIM, dtype=jnp.float32), (head_count, HEAD_DIM, HEAD_DIM)
    )
    zero_state = jnp.zeros((head_count, HEAD_DIM, HEAD_DIM), jnp.float32)
    start = jnp.concatenate([zero_state, eye_maps], axis=1)
    final, outputs = lax.scan(
        block_advance,
        start,
        (
            blocked(recept),
            blocked(decay_logarithm),
            blocked(unit_keys),
            blocked(removal),
            blocked(keyed),
            blocked(valued),
        ),
    )
    outputs = outputs.reshape(positions, head_count, 2 * HEAD_DIM)
    local_read = outputs[:, :, :HEAD_DIM]
    reached = outputs[:, :, HEAD_DIM:]
    state_end = final[:, :HEAD_DIM]
    transfer_end = final[:, HEAD_DIM:]
    prefix = entering((transfer_end, state_end), "ep", chain_join, (eye_maps, zero_state))
    head_out = local_read + jnp.einsum("hvk,thk->thv", prefix[1], reached)
    centre = jnp.mean(head_out, axis=-1, keepdims=True)
    spread = jnp.mean(jnp.square(head_out - centre), axis=-1, keepdims=True)
    normed = (head_out - centre) * lax.rsqrt(spread + group_eps)
    gated = (
        normed
        * head_norm_gain.reshape(head_count, HEAD_DIM)
        * jax.nn.sigmoid(head_view(output_gate_input))
    )
    mixed_hidden = gated.reshape(positions, head_count * HEAD_DIM).astype(jnp.bfloat16)
    summed = summed_on_arrival(
        jnp.dot(mixed_hidden, mixer_output_weight, preferred_element_type=jnp.float32).astype(
            jnp.bfloat16
        ),
        "tp",
        0,
    )
    return summed.astype(jnp.bfloat16)


def finish_experts(gate_val, up_val, expert_down_weight):
    expert_hidden = (jax.nn.silu(gate_val) * up_val).astype(jnp.bfloat16)
    summed = summed_on_arrival(
        jnp.einsum(
            "sxcf,xfd->dsxc", expert_hidden, expert_down_weight, preferred_element_type=jnp.float32
        ).astype(jnp.bfloat16),
        "tp",
        0,
    )
    return summed.astype(jnp.bfloat16)


def expert_part(
    expert_layer_input,
    feedforward_norm_gain,
    group_router_weight,
    expert_router_weight,
    routes,
    expert_gate_weight,
    expert_up_weight,
    expert_down_weight,
):
    token_rows = expert_layer_input.shape[0]
    route_count = routes.shape[1]
    ep_count = lax.axis_size("ep")
    expert_total = expert_router_weight.shape[1]
    per_group = expert_total // GROUPS
    capacity = 4 * token_rows // ep_count
    widened = expert_layer_input.astype(jnp.float32)
    normed_input = (
        widened
        * lax.rsqrt(jnp.mean(widened * widened, axis=-1, keepdims=True) + norm_eps)
        * feedforward_norm_gain
    ).astype(jnp.bfloat16)
    group_logit = jnp.dot(normed_input, group_router_weight, preferred_element_type=jnp.float32)
    group_exp = jnp.exp(group_logit)
    group_prob = group_exp / jnp.sum(group_exp, axis=-1, keepdims=True)
    expert_logit = jnp.dot(normed_input, expert_router_weight, preferred_element_type=jnp.float32)
    expert_range = jnp.arange(expert_total, dtype=jnp.int32)
    matched = routes[:, :, None] == expert_range[None, None, :]
    chosen_logit = jnp.sum(jnp.where(matched, expert_logit[:, None, :], 0.0), axis=-1)
    group_match = (routes // per_group)[:, :, None] == jnp.arange(GROUPS, dtype=jnp.int32)[
        None, None, :
    ]
    chosen_group = jnp.sum(jnp.where(group_match, group_prob[:, None, :], 0.0), axis=-1)
    route_weight = chosen_group * jax.nn.sigmoid(chosen_logit - chosen_logit[:, ::-1])
    flat_match = matched.reshape(token_rows * route_count, expert_total).astype(jnp.int32)
    before = jnp.cumsum(flat_match, axis=0) - flat_match
    placed = jnp.sum(before * flat_match, axis=1)
    slot_ids = routes.reshape(-1) * capacity + placed
    slot_range = jnp.arange(expert_total * capacity, dtype=jnp.int32)
    struck = (slot_range[:, None] == slot_ids[None, :]).reshape(
        expert_total * capacity, token_rows, route_count
    )
    dispatch_matrix = jnp.any(struck, axis=-1).astype(jnp.bfloat16)
    combine_matrix = jnp.sum(jnp.where(struck, route_weight[None, :, :], 0.0), axis=-1)
    outgoing = jnp.dot(dispatch_matrix, normed_input, preferred_element_type=jnp.float32).astype(
        jnp.bfloat16
    )
    outgoing = outgoing.reshape(ep_count, expert_total // ep_count, capacity, outgoing.shape[1])
    arrived = lax.all_to_all(outgoing, "ep", split_axis=0, concat_axis=0, tiled=True)
    gate_val = jnp.einsum(
        "sxcd,xdf->sxcf", arrived, expert_gate_weight, preferred_element_type=jnp.float32
    )
    up_val = jnp.einsum(
        "sxcd,xdf->sxcf", arrived, expert_up_weight, preferred_element_type=jnp.float32
    )
    expert_rows = finish_experts(gate_val, up_val, expert_down_weight)
    homebound = lax.all_to_all(expert_rows, "ep", split_axis=1, concat_axis=1, tiled=True)
    homebound = homebound.reshape(homebound.shape[0], expert_total * capacity)
    combined = jnp.dot(homebound.astype(jnp.float32), combine_matrix)
    return combined.T.astype(jnp.bfloat16)


def local(
    receptance,
    key_matrix,
    value_matrix,
    decay_data_term,
    correction_rate_data,
    output_gate_input,
    decay_channel_offset,
    correction_rate_offset,
    extra_head_log_decay,
    head_norm_gain,
    mixer_output_weight,
    expert_layer_input,
    feedforward_norm_gain,
    group_router_weight,
    expert_router_weight,
    routes,
    expert_gate_weight,
    expert_up_weight,
    expert_down_weight,
):
    token_mixer_output = mixer_part(
        receptance,
        key_matrix,
        value_matrix,
        decay_data_term,
        correction_rate_data,
        output_gate_input,
        decay_channel_offset,
        correction_rate_offset,
        extra_head_log_decay,
        head_norm_gain,
        mixer_output_weight,
    )
    expert_out = expert_part(
        expert_layer_input,
        feedforward_norm_gain,
        group_router_weight,
        expert_router_weight,
        routes,
        expert_gate_weight,
        expert_up_weight,
        expert_down_weight,
    )
    return (token_mixer_output, expert_out)


def solution(mesh):
    in_specs = (
        P("ep", "tp"),
        P("ep", "tp"),
        P("ep", "tp"),
        P("ep", "tp"),
        P("ep", "tp"),
        P("ep", "tp"),
        P("tp"),
        P("tp"),
        P("ep", "tp"),
        P("tp"),
        P("tp", None),
        P("ep", None),
        P(),
        P(),
        P(),
        P("ep", None),
        P("ep", None, "tp"),
        P("ep", None, "tp"),
        P("ep", "tp", None),
    )
    out_specs = (P(("ep", "tp"), None), P("ep", "tp"))
    return jax.shard_map(local, mesh=mesh, in_specs=in_specs, out_specs=out_specs, check_vma=False)
```

profile of v0, /device:TPU:1, one launch (start us, length us, event | category | flops | bytes accessed | tf_op | source)
XLA Modules:
  0.0 409.8 jit_solution(1579472441578490265)
XLA Ops:
  8.7 14.0 %all-to-all-start.2 = ((bf16[32,1,16,2048]{3,2,1,0:T(8,128)(2,1)}), bf16[32,1,16,2048]{3,2,1,0:T(8,128)(2,1)}, u32[]{:S(2)}, u32[]{:S(2)}) async-start(bf16[32,1,16,2048]{3,2,1,0:T(8,128)(2,1)} %bitcast.99), calls=%async_computation.2 | async-start | bytes 4194304 | tf_op jit(solution)/shard_map/all_to_all | solution.py:267
  28.2 226.8 %while.12 = (s32[]{:T(128)}, f32[1,128,64]{1,2,0:T(8,128)S(1)}, f32[8,64,1,128]{3,1,2,0:T(8,128)}, f32[8,64,1,64]{3,1,2,0:T(8,128)}, f32[8,64,1,64]{3,2,1,0:T(1,...) while((s32[]{:T(128)}, f32[1,128,64]{1,2,0:T(8,128)S(1)}, ...), condition=%wide.region_3.4_spmd, body=%wide.region_1.3_spmd.sunk | while | flops 18714688 | bytes 9884281 | solution.py:169
  32.9 3.3 copy.162
  36.2 4.2 %copy.166 = f32[64,64,64]{0,1,2:T(8,128)} copy(f32[64,64,64]{2,1,0:T(8,128)} %get-tuple-element.220) | data formatting | bytes 2097152 | tf_op jit(solution)/shard_map/while
  47.5 4.9 %custom-call.6 = f32[1,64,64]{1,2,0:T(8,128)S(1)} custom-call(f32[1,64,64]{2,1,0:T(8,128)S(1)} %add_bitcast_fusion.4), custom_call_target="InvertDiagBlocksLowerTriangular" | custom-call | tf_op jit(solution)/shard_map/while/body/eval_jaxpr/jit(_solve_triangular)/triangular_solve | solution.py:108
  61.2 3.3 copy.162
  64.6 4.2 %copy.166 = f32[64,64,64]{0,1,2:T(8,128)} copy(f32[64,64,64]{2,1,0:T(8,128)} %get-tuple-element.220) | data formatting | bytes 2097152 | tf_op jit(solution)/shard_map/while
  75.9 4.9 %custom-call.6 = f32[1,64,64]{1,2,0:T(8,128)S(1)} custom-call(f32[1,64,64]{2,1,0:T(8,128)S(1)} %add_bitcast_fusion.4), custom_call_target="InvertDiagBlocksLowerTriangular" | custom-call | tf_op jit(solution)/shard_map/while/body/eval_jaxpr/jit(_solve_triangular)/triangular_solve | solution.py:108
  89.6 3.3 copy.162
  92.9 4.2 %copy.166 = f32[64,64,64]{0,1,2:T(8,128)} copy(f32[64,64,64]{2,1,0:T(8,128)} %get-tuple-element.220) | data formatting | bytes 2097152 | tf_op jit(solution)/shard_map/while
  104.2 4.9 %custom-call.6 = f32[1,64,64]{1,2,0:T(8,128)S(1)} custom-call(f32[1,64,64]{2,1,0:T(8,128)S(1)} %add_bitcast_fusion.4), custom_call_target="InvertDiagBlocksLowerTriangular" | custom-call | tf_op jit(solution)/shard_map/while/body/eval_jaxpr/jit(_solve_triangular)/triangular_solve | solution.py:108
  118.0 3.3 copy.162
  121.3 4.2 %copy.166 = f32[64,64,64]{0,1,2:T(8,128)} copy(f32[64,64,64]{2,1,0:T(8,128)} %get-tuple-element.220) | data formatting | bytes 2097152 | tf_op jit(solution)/shard_map/while
  132.6 4.9 %custom-call.6 = f32[1,64,64]{1,2,0:T(8,128)S(1)} custom-call(f32[1,64,64]{2,1,0:T(8,128)S(1)} %add_bitcast_fusion.4), custom_call_target="InvertDiagBlocksLowerTriangular" | custom-call | tf_op jit(solution)/shard_map/while/body/eval_jaxpr/jit(_solve_triangular)/triangular_solve | solution.py:108
  146.3 3.3 copy.162
  149.6 4.2 %copy.166 = f32[64,64,64]{0,1,2:T(8,128)} copy(f32[64,64,64]{2,1,0:T(8,128)} %get-tuple-element.220) | data formatting | bytes 2097152 | tf_op jit(solution)/shard_map/while
  160.9 4.9 %custom-call.6 = f32[1,64,64]{1,2,0:T(8,128)S(1)} custom-call(f32[1,64,64]{2,1,0:T(8,128)S(1)} %add_bitcast_fusion.4), custom_call_target="InvertDiagBlocksLowerTriangular" | custom-call | tf_op jit(solution)/shard_map/while/body/eval_jaxpr/jit(_solve_triangular)/triangular_solve | solution.py:108
  178.0 4.2 %copy.166 = f32[64,64,64]{0,1,2:T(8,128)} copy(f32[64,64,64]{2,1,0:T(8,128)} %get-tuple-element.220) | data formatting | bytes 2097152 | tf_op jit(solution)/shard_map/while
  189.3 4.9 %custom-call.6 = f32[1,64,64]{1,2,0:T(8,128)S(1)} custom-call(f32[1,64,64]{2,1,0:T(8,128)S(1)} %add_bitcast_fusion.4), custom_call_target="InvertDiagBlocksLowerTriangular" | custom-call | tf_op jit(solution)/shard_map/while/body/eval_jaxpr/jit(_solve_triangular)/triangular_solve | solution.py:108
  206.4 4.2 %copy.166 = f32[64,64,64]{0,1,2:T(8,128)} copy(f32[64,64,64]{2,1,0:T(8,128)} %get-tuple-element.220) | data formatting | bytes 2097152 | tf_op jit(solution)/shard_map/while
  217.7 4.9 %custom-call.6 = f32[1,64,64]{1,2,0:T(8,128)S(1)} custom-call(f32[1,64,64]{2,1,0:T(8,128)S(1)} %add_bitcast_fusion.4), custom_call_target="InvertDiagBlocksLowerTriangular" | custom-call | tf_op jit(solution)/shard_map/while/body/eval_jaxpr/jit(_solve_triangular)/triangular_solve | solution.py:108
  234.7 4.2 %copy.166 = f32[64,64,64]{0,1,2:T(8,128)} copy(f32[64,64,64]{2,1,0:T(8,128)} %get-tuple-element.220) | data formatting | bytes 2097152 | tf_op jit(solution)/shard_map/while
  246.0 4.9 %custom-call.6 = f32[1,64,64]{1,2,0:T(8,128)S(1)} custom-call(f32[1,64,64]{2,1,0:T(8,128)S(1)} %add_bitcast_fusion.4), custom_call_target="InvertDiagBlocksLowerTriangular" | custom-call | tf_op jit(solution)/shard_map/while/body/eval_jaxpr/jit(_solve_triangular)/triangular_solve | solution.py:108
  256.1 9.1 %all-to-all-start = ((bf16[32,128,64]{1,2,0:T(8,128)(2,1)}), bf16[32,128,64]{1,2,0:T(8,128)(2,1)S(1)}, u32[]{:S(2)}, u32[]{:S(2)}) async-start(bf16[32,128,64]{1,2,0:T(8,128)(2,1)} %broadcast_in_dim.131), calls=%async_computation | async-start | bytes 1048576 | tf_op jit(solution)/shard_map/all_to_all | solution.py:17
  268.0 5.2 %convolution_convert_fusion = bf16[32,16,2048]{2,1,0:T(8,128)(2,1)} fusion(bf16[32,1,16,2048]{3,2,1,0:T(8,128)(2,1)} %all-to-all-done.2, bf16[1,256,2048]{2,1,0:T(8,128)(2,1)S(1)} %copy-done, bf16[1,2048,256]{2,1,0:T(8,128)(2,1)S(1)} %copy-done.20, f32[32,1,16,256]{3,2,0,1:T(8,128)S(1)} %fusion.47), kind=kOutput, calls=%fused_computation.72 | convolution fusion | flops 1075576832 | bytes 6815744 | tf_op jit(solution)/shard_map/sxcf,xfd->dsxc/dot_general | solution.py:210
  277.3 3.4 all-to-all-done
  281.5 10.4 %all-to-all-start.3 = ((bf16[16,128,32,1,16]{1,4,2,3,0:T(8,128)(2,1)}), bf16[16,128,32,1,16]{1,4,2,3,0:T(8,128)(2,1)S(1)}, u32[]{:S(2)}, u32[]{:S(2)}) async-start(bf16[16,128,32,1,16]{1,4,2,3,0:T(8,128)(2,1)} %copy.118), calls=%async_computation.3 | async-start | bytes 4194304 | tf_op jit(solution)/shard_map/all_to_all | solution.py:73
  308.9 32.1 %all-to-all-done.3 = bf16[16,128,32,1,16]{1,4,2,3,0:T(8,128)(2,1)S(1)} async-done(((bf16[16,128,32,1,16]{1,4,2,3,0:T(8,128)(2,1)}), bf16[16,128,32,1,16]{1,4,2,3,0:T(8,128)(2,1)S(1)}, u32[]{:S(2)}, u32[]{:S(2)}) %all-to-all-start.3) | async-done | bytes 2097184 | tf_op jit(solution)/shard_map/all_to_all | solution.py:73
  341.0 5.0 %all-to-all-start.1 = ((bf16[16,32,2048]{2,1,0:T(8,128)(2,1)}), bf16[16,32,2048]{2,1,0:T(8,128)(2,1)}, u32[]{:S(2)}, u32[]{:S(2)}) async-start(bf16[16,32,2048]{2,1,0:T(8,128)(2,1)} %bitcast.432), calls=%async_computation.1 | async-start | bytes 4194304 | tf_op jit(solution)/shard_map/all_to_all | solution.py:73
  349.9 45.3 %all-to-all-done.1 = bf16[16,32,2048]{2,1,0:T(8,128)(2,1)} async-done(((bf16[16,32,2048]{2,1,0:T(8,128)(2,1)}), bf16[16,32,2048]{2,1,0:T(8,128)(2,1)}, u32[]{:S(2)}, u32[]{:S(2)}) %all-to-all-start.1) | async-done | bytes 2097184 | tf_op jit(solution)/shard_map/all_to_all | solution.py:73
  395.1 4.4 %all-to-all-start.4 = ((bf16[128,32,1,16]{0,3,2,1:T(8,128)(2,1)}), bf16[128,32,1,16]{0,3,2,1:T(8,128)(2,1)S(1)}, u32[]{:S(2)}, u32[]{:S(2)}) async-start(bf16[128,32,1,16]{0,3,2,1:T(8,128)(2,1)} %bitcast.117), calls=%async_computation.4 | async-start | bytes 262144 | tf_op jit(solution)/shard_map/all_to_all | solution.py:275
  402.3 6.7 %all-to-all-done.4 = bf16[128,32,1,16]{0,3,2,1:T(8,128)(2,1)S(1)} async-done(((bf16[128,32,1,16]{0,3,2,1:T(8,128)(2,1)}), bf16[128,32,1,16]{0,3,2,1:T(8,128)(2,1)S(1)}, u32[]{:S(2)}, u32[]{:S(2)}) %all-to-all-start.4) | async-done | bytes 131104 | tf_op jit(solution)/shard_map/all_to_all | solution.py:275
  (318 shorter events, 183.5 us)
Async XLA Ops:
  0.6 267.3 %copy-start = (bf16[1,256,2048]{2,1,0:T(8,128)(2,1)S(1)}, bf16[1,256,2048]{2,1,0:T(8,128)(2,1)}, u32[]{:S(2)}) copy-start(bf16[1,256,2048]{2,1,0:T(8,128)(2,1)} %param.39) | copy-start | bytes 3145732
  4.2 1.2 copy-start.9
  5.4 3.2 copy-start.18
  8.6 14.0 %copy-start.4 = (bf16[512,64]{0,1:T(8,128)(2,1)S(1)}, bf16[512,64]{0,1:T(8,128)(2,1)}, u32[]{:S(2)}) copy-start(bf16[512,64]{0,1:T(8,128)(2,1)} %param.22) | copy-start | bytes 196612
  8.6 14.9 %copy-start.8 = (bf16[512,64]{0,1:T(8,128)(2,1)S(1)}, bf16[512,64]{0,1:T(8,128)(2,1)}, u32[]{:S(2)}) copy-start(bf16[512,64]{0,1:T(8,128)(2,1)} %param.25) | copy-start | bytes 196612
  8.6 14.9 %copy-start.16 = (f32[64]{0:T(128)S(1)}, f32[64]{0:T(128)}, u32[]{:S(2)}) copy-start(f32[64]{0:T(128)} %param.28) | copy-start | bytes 772
  8.7 16.8 %copy-start.5 = (bf16[512,64]{0,1:T(8,128)(2,1)S(1)}, bf16[512,64]{0,1:T(8,128)(2,1)}, u32[]{:S(2)}) copy-start(bf16[512,64]{0,1:T(8,128)(2,1)} %param.24) | copy-start | bytes 196612
  8.7 16.8 %copy-start.14 = (f32[512,1]{0,1:T(1,128)S(1)}, f32[512,1]{0,1:T(1,128)}, u32[]{:S(2)}) copy-start(f32[512,1]{0,1:T(1,128)} %param.29) | copy-start | bytes 6148
  8.7 16.7 %copy-start.17 = (f32[64]{0:T(128)S(1)}, f32[64]{0:T(128)}, u32[]{:S(2)}) copy-start(f32[64]{0:T(128)} %param.27) | copy-start | bytes 772
  8.7 246.5 %all-to-all-start.2 = ((bf16[32,1,16,2048]{3,2,1,0:T(8,128)(2,1)}), bf16[32,1,16,2048]{3,2,1,0:T(8,128)(2,1)}, u32[]{:S(2)}, u32[]{:S(2)}) async-start(bf16[32,1,16,2048]{3,2,1,0:T(8,128)(2,1)} %bitcast.99), calls=%async_computation.2 | async-start | bytes 4194304 | tf_op jit(solution)/shard_map/all_to_all | solution.py:267
  22.7 3.8 copy-start.6
  22.7 4.6 %copy-start.7 = (bf16[512,64]{0,1:T(8,128)(2,1)S(1)}, bf16[512,64]{0,1:T(8,128)(2,1)}, u32[]{:S(2)}) copy-start(bf16[512,64]{0,1:T(8,128)(2,1)} %param.21) | copy-start | bytes 196612
  256.1 24.6 %all-to-all-start = ((bf16[32,128,64]{1,2,0:T(8,128)(2,1)}), bf16[32,128,64]{1,2,0:T(8,128)(2,1)S(1)}, u32[]{:S(2)}, u32[]{:S(2)}) async-start(bf16[32,128,64]{1,2,0:T(8,128)(2,1)} %broadcast_in_dim.131), calls=%async_computation | async-start | bytes 1048576 | tf_op jit(solution)/shard_map/all_to_all | solution.py:17
  265.3 2.7 copy-start.20
  277.3 14.7 %copy-start.3 = (f32[8,64,1,128]{3,1,2,0:T(8,128)S(1)}, f32[8,64,1,128]{3,1,2,0:T(8,128)}, u32[]{:S(2)}) copy-start(f32[8,64,1,128]{3,1,2,0:T(8,128)} %get-tuple-element.50) | copy-start | bytes 786436
  280.7 0.8 copy-start.1
  281.5 59.5 %all-to-all-start.3 = ((bf16[16,128,32,1,16]{1,4,2,3,0:T(8,128)(2,1)}), bf16[16,128,32,1,16]{1,4,2,3,0:T(8,128)(2,1)S(1)}, u32[]{:S(2)}, u32[]{:S(2)}) async-start(bf16[16,128,32,1,16]{1,4,2,3,0:T(8,128)(2,1)} %copy.118), calls=%async_computation.3 | async-start | bytes 4194304 | tf_op jit(solution)/shard_map/all_to_all | solution.py:73
  292.7 6.5 %copy-start.15 = (pred[32]{0:T(512)(128)(4,1)}, pred[32]{0:T(512)(128)(4,1)S(1)}, u32[]{:S(2)}) copy-start(pred[32]{0:T(512)(128)(4,1)S(1)} %iota_compare_fusion.12) | copy-start | bytes 100
  299.2 1.9 copy-start.2
  341.0 5.0 %copy-start.12 = (f32[2048]{0:T(1024)S(1)}, f32[2048]{0:T(1024)}, u32[]{:S(2)}) copy-start(f32[2048]{0:T(1024)} %param.33) | copy-start | bytes 24580
  341.0 5.0 %copy-start.19 = (f32[128]{0:T(128)S(1)}, f32[128]{0:T(128)}, u32[]{:S(2)}) copy-start(f32[128]{0:T(128)} %copy-done.18) | copy-start | bytes 1540
  341.0 5.0 %copy-start.21 = (bf16[2048,32]{0,1:T(8,128)(2,1)S(1)}, bf16[2048,32]{0,1:T(8,128)(2,1)}, u32[]{:S(2)}) copy-start(bf16[2048,32]{0,1:T(8,128)(2,1)} %param.35) | copy-start | bytes 393220
  341.0 6.4 %copy-start.11 = (s32[128,2]{0,1:T(2,128)S(1)}, s32[128,2]{0,1:T(2,128)}, u32[]{:S(2)}) copy-start(s32[128,2]{0,1:T(2,128)} %param.36) | copy-start | bytes 3076
  341.0 6.5 %copy-start.22 = (bf16[2048,4]{0,1:T(4,128)(2,1)S(1)}, bf16[2048,4]{0,1:T(4,128)(2,1)}, u32[]{:S(2)}) copy-start(bf16[2048,4]{0,1:T(4,128)(2,1)} %param.34) | copy-start | bytes 49156
  341.0 7.9 %copy-start.13 = (s32[128,2]{0,1:T(2,128)S(1)}, s32[128,2]{0,1:T(2,128)}, u32[]{:S(2)}) copy-start(s32[128,2]{0,1:T(2,128)} %get-tuple-element.138) | copy-start | bytes 3076
  341.0 54.1 %all-to-all-start.1 = ((bf16[16,32,2048]{2,1,0:T(8,128)(2,1)}), bf16[16,32,2048]{2,1,0:T(8,128)(2,1)}, u32[]{:S(2)}, u32[]{:S(2)}) async-start(bf16[16,32,2048]{2,1,0:T(8,128)(2,1)} %bitcast.432), calls=%async_computation.1 | async-start | bytes 4194304 | tf_op jit(solution)/shard_map/all_to_all | solution.py:73
  346.0 53.5 %copy-start.10 = (s32[128,2]{0,1:T(2,128)S(1)}, s32[128,2]{0,1:T(2,128)}, u32[]{:S(2)}) copy-start(s32[128,2]{0,1:T(2,128)} %copy-done.9) | copy-start | bytes 3076
  395.1 13.8 %all-to-all-start.4 = ((bf16[128,32,1,16]{0,3,2,1:T(8,128)(2,1)}), bf16[128,32,1,16]{0,3,2,1:T(8,128)(2,1)S(1)}, u32[]{:S(2)}, u32[]{:S(2)}) async-start(bf16[128,32,1,16]{0,3,2,1:T(8,128)(2,1)} %bitcast.117), calls=%async_computation.4 | async-start | bytes 262144 | tf_op jit(solution)/shard_map/all_to_all | solution.py:275
where the time goes:
time: 416 us; the launch traced here: 410 us
  local copies, waits for them, and re-layouts  108 us (26%)
  other arithmetic  108 us (26%)
  waiting for transfers between devices  87.5 us (21%)
  matrix products  62.7 us (15%)
  starting transfers between devices  42.9 us (10%)
    all_to_all x2, waiting for transfers between devices, summed_on_arrival(): lax.all_to_all(parts, axis, split_axis=0, concat_axis=0, tiled=True)  77.3 us
    while x16, local copies, waits for them, and re-layouts  59.9 us
    another operation x24, other arithmetic, block_advance(): jax.scipy.linalg.solve_triangular(left_side, right_side, lower=True, unit...  39.9 us
    while x8, other arithmetic  25.8 us
    select_n x8, other arithmetic, pair_decay(): return jnp.where(mask, jnp.exp(jnp.where(mask, gap, 0.0)), 0.0)  24.7 us
    all_to_all x2, starting transfers between devices, summed_on_arrival(): lax.all_to_all(parts, axis, split_axis=0, concat_axis=0, tiled=True)  15.4 us
    another operation x50, local copies, waits for them, and re-layouts  15.2 us
    all_to_all x1, starting transfers between devices, expert_part(): lax.all_to_all(outgoing, 'ep', split_axis=0, concat_axis=0, tiled=True)  14 us
  transfers between devices with their start and end apart: 5, of which 4 were waited for; matrix products, arithmetic and copies ran while one was open for 65% of the time, Pallas kernels for 0%

commit v1 on v0

--- a/solution.py
+++ b/solution.py
@@ -1,6 +1,9 @@
+import functools
 import jax
 import jax.numpy as jnp
 from jax import lax
+from jax.experimental import pallas as pl
+from jax.experimental.pallas import tpu as pltpu
 from jax.sharding import PartitionSpec as P
 
 HEAD_DIM = 64
@@ -74,52 +77,99 @@
     return arrived.astype(jnp.float32).sum(axis=0)
 
 
+HD=64
+f32=jnp.float32; bf16=jnp.bfloat16
+NN=(((1,),(0,)),((),())); NT=(((1,),(1,)),((),())); TN=(((0,),(0,)),((),()))
+def dotb(a,b,dims=NN):
+    return lax.dot_general(a.astype(bf16), b.astype(bf16), dims, preferred_element_type=f32)
+def dot3(a,b,dims=NN):
+    ah=a.astype(bf16); bh=b.astype(bf16)
+    al=(a-ah.astype(f32)).astype(bf16); bl=(b-bh.astype(f32)).astype(bf16)
+    d=lambda p,q: lax.dot_general(p,q,dims,preferred_element_type=f32)
+    return d(ah,bh)+(d(ah,bl)+d(al,bh))
+def dot2(a,b,dims=NN):
+    ah=a.astype(bf16); bh=b.astype(bf16); bl=(b-bh.astype(f32)).astype(bf16)
+    d=lambda p,q: lax.dot_general(p,q,dims,preferred_element_type=f32)
+    return d(ah,bh)+d(ah,bl)
+def sigmoid(x): return 1.0/(1.0+jnp.exp(-x))
+def chunk_local(r,k,v,dd,cr,doff,coff,extra, inv_dot=dot3):
+    C=r.shape[0]
+    row=lax.broadcasted_iota(jnp.int32,(C,C),0); col=lax.broadcasted_iota(jnp.int32,(C,C),1)
+    u=k*lax.rsqrt(jnp.sum(k*k,axis=-1,keepdims=True)+1e-6)
+    a=u*sigmoid(cr+coff)
+    lg=extra-0.6065306597126334*sigmoid(dd+doff)
+    tri=jnp.where(row>=col,1.0,0.0)
+    lh=lg.astype(bf16); l2=lg-lh.astype(f32); lm=l2.astype(bf16); ll=(l2-lm.astype(f32)).astype(bf16)
+    tb=tri.astype(bf16)
+    d=lambda q: lax.dot_general(tb,q,NN,preferred_element_type=f32)
+    cum=d(lh)+(d(lm)+d(ll))
+    bef=cum-lg
+    tot=cum[C-1:C,:]
+    ref=0.5*tot
+    en=jnp.exp(ref-cum)
+    lhs=jnp.concatenate([u*jnp.exp(bef-ref), r*jnp.exp(cum-ref)],axis=0)
+    rhs=jnp.concatenate([k*en, a*en],axis=0)
+    G=dotb(lhs,rhs,NT)
+    strict=row>col; upto=row>=col
+    kp=jnp.where(strict,G[:C,:C],0.0); A=jnp.where(strict,G[:C,C:],0.0)
+    rk=jnp.where(upto,G[C:,:C],0.0); rr=jnp.where(upto,G[C:,C:],0.0)
+    x=row^col
+    T=jnp.where(row==col,1.0,0.0)-jnp.where(x==1,A,0.0)
+    s=2
+    while s<C:
+        m=jnp.where((x>=s)&(x<2*s),A,0.0)
+        T=T-inv_dot(T,inv_dot(m,T))
+        s*=2
+    kv=dotb(jnp.concatenate([kp,rk],axis=0),v)
+    R=jnp.concatenate([kv[:C],u*jnp.exp(bef)],axis=1)
+    X=dotb(T,R)
+    out=jnp.concatenate([kv[C:],r*jnp.exp(cum)],axis=1)-dotb(rr,X)
+    tail=jnp.exp(tot-cum)
+    r64=lax.broadcasted_iota(jnp.int32,(HD,HD),0); c64=lax.broadcasted_iota(jnp.int32,(HD,HD),1)
+    diag=jnp.where(r64==c64,jnp.exp(tot),0.0)
+    BM=jnp.concatenate([dotb(k*tail,v,TN),diag],axis=1)-dotb(a*tail,X,TN)
+    return out,BM
+
 def chain_join(earlier, later):
-    joined_map = jnp.einsum("hvk,hkj->hvj", earlier[0], later[0])
-    joined_state = jnp.einsum("hvk,hkj->hvj", earlier[1], later[0]) + later[1]
+    joined_map = jnp.einsum("vk,kj->vj", later[0], earlier[0])
+    joined_state = jnp.einsum("vk,kj->vj", later[0], earlier[1]) + later[1]
     return (joined_map, joined_state)
 
 
-def pair_decay(upper, lower, keep):
-    gap = upper[:, None] - lower[None, :]
-    mask = keep[:, :, None, None]
-    return jnp.where(mask, jnp.exp(jnp.where(mask, gap, 0.0)), 0.0)
-
-
-def block_advance(stacked, inputs):
-    recept_b, log_b, unit_b, removal_b, key_b, value_b = inputs
-    block_len = recept_b.shape[0]
-    cumul = jnp.cumsum(log_b, axis=0)
-    before = cumul - log_b
-    places = jnp.arange(block_len)
-    strict = places[:, None] > places[None, :]
-    upto = places[:, None] >= places[None, :]
-    strict_decay = pair_decay(before, cumul, strict)
-    upto_decay = pair_decay(cumul, cumul, upto)
-    key_pairs = jnp.einsum("jhk,ihk,jihk->hji", unit_b, key_b, strict_decay)
-    removal_pairs = jnp.einsum("jhk,ihk,jihk->hji", unit_b, removal_b, strict_decay)
-    read_keys = jnp.einsum("thk,ihk,tihk->hti", recept_b, key_b, upto_decay)
-    read_removal = jnp.einsum("thk,ihk,tihk->hti", recept_b, removal_b, upto_decay)
-    value_padded = jnp.concatenate([value_b, jnp.zeros_like(value_b)], axis=-1)
-    right_side = jnp.einsum("jhk,hrk->hjr", unit_b * jnp.exp(before), stacked) + jnp.einsum(
-        "hji,ihr->hjr", key_pairs, value_padded
-    )
-    left_side = jnp.eye(block_len, dtype=jnp.float32)[None] + removal_pairs
-    corrected = jax.scipy.linalg.solve_triangular(
-        left_side, right_side, lower=True, unit_diagonal=True
-    )
-    outputs = (
-        jnp.einsum("thk,hrk->thr", recept_b * jnp.exp(cumul), stacked)
-        + jnp.einsum("hti,ihr->thr", read_keys, value_padded)
-        - jnp.einsum("hti,hir->thr", read_removal, corrected)
-    )
-    tail = jnp.exp(cumul[-1][None] - cumul)
-    stacked = (
-        stacked * jnp.exp(cumul[-1])[:, None, :]
-        + jnp.einsum("ihr,ihk->hrk", value_padded, key_b * tail)
-        - jnp.einsum("hir,ihk->hrk", corrected, removal_b * tail)
-    )
-    return (stacked, outputs)
+def local_kernel(r, k, v, dd, cr, doff, coff, extra, out_ref, qp_ref, dev_ref):
+    C = 128
+    parts = []
+    for c in range(4):
+        s = slice(c * C, (c + 1) * C)
+        out, bm = chunk_local(
+            r[s].astype(f32), k[s].astype(f32), v[s].astype(f32), dd[s].astype(f32),
+            cr[s].astype(f32), doff[...], coff[...], extra[s],
+        )
+        out_ref[s] = out
+        parts.append(bm)
+    r64 = lax.broadcasted_iota(jnp.int32, (HD, 2 * HD), 0)
+    c64 = lax.broadcasted_iota(jnp.int32, (HD, 2 * HD), 1)
+    qp = jnp.where(c64 == r64 + HD, 1.0, 0.0)
+    for c in range(4):
+        qp_ref[c] = qp
+        bm = parts[c]
+        qp = dot3(bm[:, HD:], qp) + jnp.where(c64 < HD, bm, 0.0)
+    dev_ref[...] = qp.astype(bf16)
+
+
+def finish_kernel(out_ref, qp_ref, z_ref, gate, gain, mixed_ref):
+    C = 128
+    z = z_ref[...]
+    for c in range(4):
+        s = slice(c * C, (c + 1) * C)
+        qp = qp_ref[c]
+        zc = dot2(qp[:, HD:], z) + qp[:, :HD]
+        out = out_ref[s]
+        ho = out[:, :HD] + dotb(out[:, HD:], zc)
+        ho = ho - jnp.mean(ho, axis=-1, keepdims=True)
+        sp = jnp.mean(ho * ho, axis=-1, keepdims=True)
+        g = sigmoid(gate[s].astype(f32))
+        mixed_ref[s] = (ho * lax.rsqrt(sp + group_eps) * gain[...] * g).astype(bf16)
 
 
 def mixer_part(
@@ -135,65 +185,23 @@
     head_norm_gain,
     mixer_output_weight,
 ):
-    positions = receptance.shape[0]
-    head_count = receptance.shape[1] // HEAD_DIM
-
-    def head_view(tensor_in):
-        return tensor_in.astype(jnp.float32).reshape(positions, head_count, HEAD_DIM)
-
-    recept = head_view(receptance)
-    keyed = head_view(key_matrix)
-    valued = head_view(value_matrix)
-    unit_keys = keyed * lax.rsqrt(jnp.sum(keyed * keyed, axis=-1, keepdims=True) + key_eps)
-    learn_rate = jax.nn.sigmoid(
-        head_view(correction_rate_data) + correction_rate_offset.reshape(head_count, HEAD_DIM)
-    )
-    decay_preactivation = head_view(decay_data_term) + decay_channel_offset.reshape(
-        head_count, HEAD_DIM
-    )
-    decay_logarithm = (
-        -jnp.exp(-jax.nn.softplus(-decay_preactivation) - 0.5) + extra_head_log_decay[:, :, None]
-    )
-    removal = unit_keys * learn_rate
-    block_len = min(64, positions)
-    block_count = positions // block_len
-
-    def blocked(tensor_in):
-        return tensor_in.reshape(block_count, block_len, head_count, HEAD_DIM)
-
-    eye_maps = jnp.broadcast_to(
-        jnp.eye(HEAD_DIM, dtype=jnp.float32), (head_count, HEAD_DIM, HEAD_DIM)
-    )
-    zero_state = jnp.zeros((head_count, HEAD_DIM, HEAD_DIM), jnp.float32)
-    start = jnp.concatenate([zero_state, eye_maps], axis=1)
-    final, outputs = lax.scan(
-        block_advance,
-        start,
-        (
-            blocked(recept),
-            blocked(decay_logarithm),
-            blocked(unit_keys),
-            blocked(removal),
-            blocked(keyed),
-            blocked(valued),
+    rows = receptance.shape[0]
+    out, qp, dev = pl.pallas_call(
+        local_kernel,
+        out_shape=(
+            jax.ShapeDtypeStruct((rows, 2 * HD), f32),
+            jax.ShapeDtypeStruct((4, HD, 2 * HD), f32),
+            jax.ShapeDtypeStruct((HD, 2 * HD), bf16),
         ),
-    )
-    outputs = outputs.reshape(positions, head_count, 2 * HEAD_DIM)
-    local_read = outputs[:, :, :HEAD_DIM]
-    reached = outputs[:, :, HEAD_DIM:]
-    state_end = final[:, :HEAD_DIM]
-    transfer_end = final[:, HEAD_DIM:]
-    prefix = entering((transfer_end, state_end), "ep", chain_join, (eye_maps, zero_state))
-    head_out = local_read + jnp.einsum("hvk,thk->thv", prefix[1], reached)
-    centre = jnp.mean(head_out, axis=-1, keepdims=True)
-    spread = jnp.mean(jnp.square(head_out - centre), axis=-1, keepdims=True)
-    normed = (head_out - centre) * lax.rsqrt(spread + group_eps)
-    gated = (
-        normed
-        * head_norm_gain.reshape(head_count, HEAD_DIM)
-        * jax.nn.sigmoid(head_view(output_gate_input))
-    )
-    mixed_hidden = gated.reshape(positions, head_count * HEAD_DIM).astype(jnp.bfloat16)
+    )(
+        receptance, key_matrix, value_matrix, decay_data_term, correction_rate_data,
+        decay_channel_offset.reshape(1, HD), correction_rate_offset.reshape(1, HD), extra_head_log_decay,
+    )
+    zero = jnp.zeros((HD, HD), f32)
+    prefix = entering((dev[:, HD:].astype(f32), dev[:, :HD].astype(f32)), "ep", chain_join, (jnp.eye(HD, dtype=f32), zero))
+    mixed_hidden = pl.pallas_call(
+        finish_kernel, out_shape=jax.ShapeDtypeStruct((rows, HD), bf16)
+    )(out, qp, prefix[1], output_gate_input, head_norm_gain.reshape(1, HD))
     summed = summed_on_arrival(
         jnp.dot(mixed_hidden, mixer_output_weight, preferred_element_type=jnp.float32).astype(
             jnp.bfloat16

time: 416 us -> 225 us (0.54); the launches traced: 410 us -> 224 us
  other arithmetic: 108 us -> 7.95 us
  local copies, waits for them, and re-layouts: 108 us -> 20.9 us
  matrix products: 62.7 us -> 19.6 us
  waiting for transfers between devices: 87.5 us -> 119 us
  Pallas kernels: 0 us -> 14.6 us
    while x19 -> x0, local copies, waits for them, and re-layouts: 62.4 us -> none
    dot_general x64 -> x8, matrix products: 43 us -> 1.93 us  [the longest x5 1.41 us: chain_join(): joined_state = jnp.einsum('vk,kj->vj', later[0], earlier[1]) + later[1]]
    another operation x35 -> x2, other arithmetic: 41.1 us -> 0.63 us  [the longest x24 39.9 us: block_advance(): jax.scipy.linalg.solve_triangular(left_side, right_side, lower=True, unit...]
    all_to_all x1, waiting for transfers between devices: 0.01 us -> 30.5 us  [expert_part(): lax.all_to_all(outgoing, 'ep', split_axis=0, concat_axis=0, tiled=True)]
    while x8 -> x0, other arithmetic: 25.8 us -> none
    select_n x8 -> x0, other arithmetic: 24.7 us -> none  [pair_decay(): return jnp.where(mask, jnp.exp(jnp.where(mask, gap, 0.0)), 0.0)]
    another operation x52 -> x1, local copies, waits for them, and re-layouts: 16.9 us -> 0.01 us
    pallas_call x0 -> x2, Pallas kernels: none -> 14.6 us  [the longest x1 12.3 us: mixer_part(): pl.pallas_call(local_kernel, out_shape=(jax.ShapeDtypeStruct((rows, 2 * H...]
  transfers between devices with their start and end apart: 5 -> 5, of which waited for: 4 -> 5; matrix products, arithmetic and copies ran while one was open for 65% -> 17% of each run, Pallas kernels for 0% -> 7%
where the time goes in v1:
time: 225 us; the launch traced here: 224 us
  waiting for transfers between devices  119 us (53%)
  starting transfers between devices  40.9 us (18%)
  local copies, waits for them, and re-layouts  20.9 us (9%)
  matrix products  19.6 us (9%)
  Pallas kernels  14.6 us (6%)
  other arithmetic  7.95 us (4%)
    all_to_all x2, waiting for transfers between devices, summed_on_arrival(): lax.all_to_all(parts, axis, split_axis=0, concat_axis=0, tiled=True)  78.3 us
    all_to_all x1, waiting for transfers between devices, expert_part(): lax.all_to_all(outgoing, 'ep', split_axis=0, concat_axis=0, tiled=True)  30.5 us
    all_to_all x2, starting transfers between devices, summed_on_arrival(): lax.all_to_all(parts, axis, split_axis=0, concat_axis=0, tiled=True)  15.8 us
    unnamed x45, local copies, waits for them, and re-layouts  14 us
    all_to_all x1, starting transfers between devices, expert_part(): lax.all_to_all(outgoing, 'ep', split_axis=0, concat_axis=0, tiled=True)  13.8 us
    pallas_call x1, Pallas kernels, mixer_part(): pl.pallas_call(local_kernel, out_shape=(jax.ShapeDtypeStruct((rows, 2 * H...  12.3 us
    all_to_all x1, waiting for transfers between devices, expert_part(): lax.all_to_all(expert_rows, 'ep', split_axis=1, concat_axis=1, tiled=True)  6.7 us
    all_to_all x1, starting transfers between devices, sent_to_all(): lax.all_to_all(jnp.broadcast_to(value[None], (devices, *value.shape)), ax...  6.67 us
  transfers between devices with their start and end apart: 5, of which 5 were waited for; matrix products, arithmetic and copies ran while one was open for 17% of the time, Pallas kernels for 7%

profile of v1, /device:TPU:1, one launch (start us, length us, event | category | flops | bytes accessed | tf_op | source)
XLA Modules:
  0.0 223.6 jit_solution(11846627196011622515)
XLA Ops:
  0.6 0.9 copy.98
  1.8 1.2 fusion.23
  5.0 3.2 %convolution_convert_fusion.1 = bf16[512,2048]{1,0:T(8,128)(2,1)} fusion(pred[512,128]{1,0:T(8,128)(4,1)S(1)} %fusion.35, bf16[128,2048]{1,0:T(8,128)(2,1)} %param.30, f32[2048]{0:T(1024)} %param.31, f32[128]{0:T(128)S(1)} %add_rsqrt_fusion), kind=kOutput, calls=%fused_computation.1 | convolution fusion | flops 270532608 | bytes 2695680 | tf_op jit(solution)/shard_map/dot_general | solution.py:271
  8.2 13.8 %all-to-all-start.2 = ((bf16[32,1,16,2048]{3,2,1,0:T(8,128)(2,1)}), bf16[32,1,16,2048]{3,2,1,0:T(8,128)(2,1)S(1)}, u32[]{:S(2)}, u32[]{:S(2)}) async-start(bf16[32,1,16,2048]{3,2,1,0:T(8,128)(2,1)} %bitcast.10), calls=%async_computation.2 | async-start | bytes 4194304 | tf_op jit(solution)/shard_map/all_to_all | solution.py:275
  25.8 0.9 copy.93.extra
  26.7 12.3 %shard_map.194 = (f32[512,128]{1,0:T(8,128)}, f32[4,64,128]{2,1,0:T(8,128)}, bf16[64,128]{1,0:T(8,128)(2,1)}) custom-call(bf16[512,64]{1,0:T(8,128)(2,1)} %copy.88.r, bf16[512,64]{1,0:T(8,128)(2,1)} %copy.89.k, bf16[512,64]{1,0:T(8,128)(2,1)} %copy.90.v, bf16[512,64]{1,0:T(8,128)(2,1)} %copy.91.dd, bf16[512,64]{1,0:T(8,128)(2,1)} %copy.92.cr, ...), custom_call_target="tpu_custom_call" | custom-call | tf_op jit(solution)/shard_map/pallas_call | solution.py:189
  39.1 0.9 fusion.67
  40.0 30.5 %all-to-all-done.2 = bf16[32,1,16,2048]{3,2,1,0:T(8,128)(2,1)S(1)} async-done(((bf16[32,1,16,2048]{3,2,1,0:T(8,128)(2,1)}), bf16[32,1,16,2048]{3,2,1,0:T(8,128)(2,1)S(1)}, u32[]{:S(2)}, u32[]{:S(2)}) %all-to-all-start.2) | async-done | bytes 2097184 | tf_op jit(solution)/shard_map/all_to_all | solution.py:275
  70.5 1.0 broadcast_in_dim.74
  72.0 6.7 %all-to-all-start = ((bf16[32,128,64]{1,2,0:T(8,128)(2,1)}), bf16[32,128,64]{1,2,0:T(8,128)(2,1)S(1)}, u32[]{:S(2)}, u32[]{:S(2)}) async-start(bf16[32,128,64]{1,2,0:T(8,128)(2,1)} %broadcast_in_dim.74), calls=%async_computation | async-start | bytes 1048576 | tf_op jit(solution)/shard_map/all_to_all | solution.py:20
  78.7 2.7 %fusion.4 = f32[32,1,16,256]{3,2,0,1:T(8,128)S(1)} fusion(bf16[32,1,16,2048]{3,2,1,0:T(8,128)(2,1)} %copy-done.2, bf16[1,2048,256]{2,1,0:T(8,128)(2,1)} %param.35), kind=kOutput, calls=%fused_computation.9 | convolution fusion | flops 536870912 | bytes 3670016 | tf_op jit(solution)/shard_map/sxcd,xdf->sxcf/dot_general | solution.py:276
  81.4 5.2 %convolution_convert_fusion = bf16[32,16,2048]{2,1,0:T(8,128)(2,1)} fusion(bf16[32,1,16,2048]{3,2,1,0:T(8,128)(2,1)} %copy-done.2, bf16[1,256,2048]{2,1,0:T(8,128)(2,1)S(1)} %copy-done, bf16[1,2048,256]{2,1,0:T(8,128)(2,1)S(1)} %copy-done.14, f32[32,1,16,256]{3,2,0,1:T(8,128)S(1)} %fusion.4), kind=kOutput, calls=%fused_computation | convolution fusion | flops 1075576832 | bytes 6815744 | tf_op jit(solution)/shard_map/sxcf,xfd->dsxc/dot_general | solution.py:218
  86.6 2.2 copy.107
  88.8 1.9 copy.103
  90.7 3.2 %all-to-all-done = bf16[32,128,64]{1,2,0:T(8,128)(2,1)S(1)} async-done(((bf16[32,128,64]{1,2,0:T(8,128)(2,1)}), bf16[32,128,64]{1,2,0:T(8,128)(2,1)S(1)}, u32[]{:S(2)}, u32[]{:S(2)}) %all-to-all-start) | async-done | bytes 524320 | tf_op jit(solution)/shard_map/all_to_all | solution.py:20
  94.7 10.8 %all-to-all-start.3 = ((bf16[16,128,32,1,16]{1,4,2,3,0:T(8,128)(2,1)}), bf16[16,128,32,1,16]{1,4,2,3,0:T(8,128)(2,1)S(1)}, u32[]{:S(2)}, u32[]{:S(2)}) async-start(bf16[16,128,32,1,16]{1,4,2,3,0:T(8,128)(2,1)} %copy.103), calls=%async_computation.3 | async-start | bytes 4194304 | tf_op jit(solution)/shard_map/all_to_all | solution.py:76
  106.2 2.4 %fusion.66 = (bf16[32,64,64]{1,2,0:T(8,128)(2,1)}, bf16[32,64,64]{1,2,0:T(8,128)(2,1)}) fusion(bf16[32,128,64]{1,2,0:T(8,128)(2,1)} %copy-done.1), kind=kLoop, calls=%fused_computation.88 | loop fusion | bytes 1048576 | tf_op jit(solution)/shard_map/slice | solution.py:35
  108.6 2.1 copy.105
  110.7 2.0 copy.104
  112.7 1.3 convert_select_fusion.1
  116.3 2.3 %shard_map.195 = bf16[512,64]{1,0:T(8,128)(2,1)} custom-call(f32[512,128]{1,0:T(8,128)} %get-tuple-element.5.out_ref, f32[4,64,128]{2,1,0:T(8,128)} %get-tuple-element.6.qp_ref, f32[64,64]{1,0:T(8,128)} %fusion.20.z_ref, bf16[512,64]{1,0:T(8,128)(2,1)} %copy.97.gate, f32[1,64]{1,0:T(1,128)} %bitcast.116), custom_call_target="tpu_custom_call" | custom-call | tf_op jit(solution)/shard_map/pallas_call | solution.py:202
  118.6 2.9 %convolution_convert_fusion.2 = bf16[512,2048]{1,0:T(8,128)(2,1)} fusion(bf16[512,64]{1,0:T(8,128)(2,1)} %shard_map.195, bf16[64,2048]{1,0:T(8,128)(2,1)S(1)} %copy-done.4), kind=kOutput, calls=%fused_computation.2 | convolution fusion | flops 135266304 | bytes 2424832 | tf_op jit(solution)/shard_map/dot_general | solution.py:206
  121.5 33.0 %all-to-all-done.3 = bf16[16,128,32,1,16]{1,4,2,3,0:T(8,128)(2,1)S(1)} async-done(((bf16[16,128,32,1,16]{1,4,2,3,0:T(8,128)(2,1)}), bf16[16,128,32,1,16]{1,4,2,3,0:T(8,128)(2,1)S(1)}, u32[]{:S(2)}, u32[]{:S(2)}) %all-to-all-start.3) | async-done | bytes 2097184 | tf_op jit(solution)/shard_map/all_to_all | solution.py:76
  154.5 5.0 %all-to-all-start.1 = ((bf16[16,32,2048]{2,1,0:T(8,128)(2,1)}), bf16[16,32,2048]{2,1,0:T(8,128)(2,1)}, u32[]{:S(2)}, u32[]{:S(2)}) async-start(bf16[16,32,2048]{2,1,0:T(8,128)(2,1)} %bitcast.110), calls=%async_computation.1 | async-start | bytes 4194304 | tf_op jit(solution)/shard_map/all_to_all | solution.py:76
  159.5 1.4 fusion.63
  161.0 1.4 fusion.68
  162.4 1.0 reduce_sum.90
  163.3 45.3 %all-to-all-done.1 = bf16[16,32,2048]{2,1,0:T(8,128)(2,1)} async-done(((bf16[16,32,2048]{2,1,0:T(8,128)(2,1)}), bf16[16,32,2048]{2,1,0:T(8,128)(2,1)}, u32[]{:S(2)}, u32[]{:S(2)}) %all-to-all-start.1) | async-done | bytes 2097184 | tf_op jit(solution)/shard_map/all_to_all | solution.py:76
  208.6 4.6 %all-to-all-start.4 = ((bf16[128,32,1,16]{0,3,2,1:T(8,128)(2,1)}), bf16[128,32,1,16]{0,3,2,1:T(8,128)(2,1)S(1)}, u32[]{:S(2)}, u32[]{:S(2)}) async-start(bf16[128,32,1,16]{0,3,2,1:T(8,128)(2,1)} %bitcast.28), calls=%async_computation.4 | async-start | bytes 262144 | tf_op jit(solution)/shard_map/all_to_all | solution.py:283
  213.3 2.7 %reduce_sum.82 = bf16[32,2048]{1,0:T(8,128)(2,1)} reduce(bf16[16,32,2048]{2,1,0:T(8,128)(2,1)} %all-to-all-done.1, bf16[]{:T(256)} %constant.35.clone.1), dimensions={0}, to_apply=%region_0.1 | reduce | flops 983040 | bytes 2228226 | tf_op jit(solution)/shard_map/reduce_sum | solution.py:77
  216.0 6.7 %all-to-all-done.4 = bf16[128,32,1,16]{0,3,2,1:T(8,128)(2,1)S(1)} async-done(((bf16[128,32,1,16]{0,3,2,1:T(8,128)(2,1)}), bf16[128,32,1,16]{0,3,2,1:T(8,128)(2,1)S(1)}, u32[]{:S(2)}, u32[]{:S(2)}) %all-to-all-start.4) | async-done | bytes 131104 | tf_op jit(solution)/shard_map/all_to_all | solution.py:283
  222.7 0.8 fusion.69
  (73 shorter events, 10.6 us)
Async XLA Ops:
  0.6 80.7 %copy-start = (bf16[1,256,2048]{2,1,0:T(8,128)(2,1)S(1)}, bf16[1,256,2048]{2,1,0:T(8,128)(2,1)}, u32[]{:S(2)}) copy-start(bf16[1,256,2048]{2,1,0:T(8,128)(2,1)} %param.37) | copy-start | bytes 3145732
  8.1 13.9 %copy-start.5 = (bf16[512,64]{0,1:T(8,128)(2,1)S(1)}, bf16[512,64]{0,1:T(8,128)(2,1)}, u32[]{:S(2)}) copy-start(bf16[512,64]{0,1:T(8,128)(2,1)} %param.19) | copy-start | bytes 196612
  8.1 14.7 %copy-start.6 = (bf16[512,64]{0,1:T(8,128)(2,1)S(1)}, bf16[512,64]{0,1:T(8,128)(2,1)}, u32[]{:S(2)}) copy-start(bf16[512,64]{0,1:T(8,128)(2,1)} %param.20) | copy-start | bytes 196612
  8.1 15.4 %copy-start.7 = (bf16[512,64]{0,1:T(8,128)(2,1)S(1)}, bf16[512,64]{0,1:T(8,128)(2,1)}, u32[]{:S(2)}) copy-start(bf16[512,64]{0,1:T(8,128)(2,1)} %param.21) | copy-start | bytes 196612
  8.1 16.2 %copy-start.8 = (bf16[512,64]{0,1:T(8,128)(2,1)S(1)}, bf16[512,64]{0,1:T(8,128)(2,1)}, u32[]{:S(2)}) copy-start(bf16[512,64]{0,1:T(8,128)(2,1)} %param.22) | copy-start | bytes 196612
  8.2 16.9 %copy-start.9 = (bf16[512,64]{0,1:T(8,128)(2,1)S(1)}, bf16[512,64]{0,1:T(8,128)(2,1)}, u32[]{:S(2)}) copy-start(bf16[512,64]{0,1:T(8,128)(2,1)} %param.23) | copy-start | bytes 196612
  8.2 17.7 %copy-start.13 = (f32[512,1]{0,1:T(1,128)S(1)}, f32[512,1]{0,1:T(1,128)}, u32[]{:S(2)}) copy-start(f32[512,1]{0,1:T(1,128)} %param.27) | copy-start | bytes 6148
  8.2 62.3 %all-to-all-start.2 = ((bf16[32,1,16,2048]{3,2,1,0:T(8,128)(2,1)}), bf16[32,1,16,2048]{3,2,1,0:T(8,128)(2,1)S(1)}, u32[]{:S(2)}, u32[]{:S(2)}) async-start(bf16[32,1,16,2048]{3,2,1,0:T(8,128)(2,1)} %bitcast.10), calls=%async_computation.2 | async-start | bytes 4194304 | tf_op jit(solution)/shard_map/all_to_all | solution.py:275
  70.5 1.5 copy-start.2
  72.0 21.8 %all-to-all-start = ((bf16[32,128,64]{1,2,0:T(8,128)(2,1)}), bf16[32,128,64]{1,2,0:T(8,128)(2,1)S(1)}, u32[]{:S(2)}, u32[]{:S(2)}) async-start(bf16[32,128,64]{1,2,0:T(8,128)(2,1)} %broadcast_in_dim.74), calls=%async_computation | async-start | bytes 1048576 | tf_op jit(solution)/shard_map/all_to_all | solution.py:20
  78.7 2.7 %copy-start.14 = (bf16[1,2048,256]{2,1,0:T(8,128)(2,1)S(1)}, bf16[1,2048,256]{2,1,0:T(8,128)(2,1)}, u32[]{:S(2)}) copy-start(bf16[1,2048,256]{2,1,0:T(8,128)(2,1)} %param.36) | copy-start | bytes 3145732
  90.7 14.7 %copy-start.10 = (bf16[512,64]{0,1:T(8,128)(2,1)S(1)}, bf16[512,64]{0,1:T(8,128)(2,1)}, u32[]{:S(2)}) copy-start(bf16[512,64]{0,1:T(8,128)(2,1)} %param.24) | copy-start | bytes 196612
  93.9 0.8 copy-start.1
  94.7 59.8 %all-to-all-start.3 = ((bf16[16,128,32,1,16]{1,4,2,3,0:T(8,128)(2,1)}), bf16[16,128,32,1,16]{1,4,2,3,0:T(8,128)(2,1)S(1)}, u32[]{:S(2)}, u32[]{:S(2)}) async-start(bf16[16,128,32,1,16]{1,4,2,3,0:T(8,128)(2,1)} %copy.103), calls=%async_computation.3 | async-start | bytes 4194304 | tf_op jit(solution)/shard_map/all_to_all | solution.py:76
  112.7 1.9 copy-start.3
  114.7 3.9 %copy-start.4 = (bf16[64,2048]{1,0:T(8,128)(2,1)S(1)}, bf16[64,2048]{1,0:T(8,128)(2,1)}, u32[]{:S(2)}) copy-start(bf16[64,2048]{1,0:T(8,128)(2,1)} %param.29) | copy-start | bytes 786436
  154.5 5.0 %copy-start.12 = (f32[2048]{0:T(1024)S(1)}, f32[2048]{0:T(1024)}, u32[]{:S(2)}) copy-start(f32[2048]{0:T(1024)} %param.31) | copy-start | bytes 24580
  154.5 5.0 %copy-start.15 = (bf16[2048,32]{0,1:T(8,128)(2,1)S(1)}, bf16[2048,32]{0,1:T(8,128)(2,1)}, u32[]{:S(2)}) copy-start(bf16[2048,32]{0,1:T(8,128)(2,1)} %param.33) | copy-start | bytes 393220
  154.5 6.4 %copy-start.11 = (s32[128,2]{0,1:T(2,128)S(1)}, s32[128,2]{0,1:T(2,128)}, u32[]{:S(2)}) copy-start(s32[128,2]{0,1:T(2,128)} %param.34) | copy-start | bytes 3076
  154.5 6.5 %copy-start.16 = (bf16[2048,4]{0,1:T(4,128)(2,1)S(1)}, bf16[2048,4]{0,1:T(4,128)(2,1)}, u32[]{:S(2)}) copy-start(bf16[2048,4]{0,1:T(4,128)(2,1)} %param.32) | copy-start | bytes 49156
  154.5 54.1 %all-to-all-start.1 = ((bf16[16,32,2048]{2,1,0:T(8,128)(2,1)}), bf16[16,32,2048]{2,1,0:T(8,128)(2,1)}, u32[]{:S(2)}, u32[]{:S(2)}) async-start(bf16[16,32,2048]{2,1,0:T(8,128)(2,1)} %bitcast.110), calls=%async_computation.1 | async-start | bytes 4194304 | tf_op jit(solution)/shard_map/all_to_all | solution.py:76
  208.6 14.1 %all-to-all-start.4 = ((bf16[128,32,1,16]{0,3,2,1:T(8,128)(2,1)}), bf16[128,32,1,16]{0,3,2,1:T(8,128)(2,1)S(1)}, u32[]{:S(2)}, u32[]{:S(2)}) async-start(bf16[128,32,1,16]{0,3,2,1:T(8,128)(2,1)} %bitcast.28), calls=%async_computation.4 | async-start | bytes 262144 | tf_op jit(solution)/shard_map/all_to_all | solution.py:283

commit v2 on v0

v2 whole, which is shorter than its diff:
```python
import jax
import jax.numpy as jnp
from jax import lax
from jax.experimental import pallas as pl
from jax.experimental.pallas import tpu as pltpu
from jax.sharding import PartitionSpec as P

f32 = jnp.float32
bf16 = jnp.bfloat16
MESH = pl.DeviceIdType.MESH
HD = 64
CH = 128
NX, NZ, NY = 4, 8, 8
CAP = 16
GROUPS = 4
key_eps = 1e-06
group_eps = 0.00064
norm_eps = 1e-06
HALF = 4
ROWS = 256 // HALF

NN = (((1,), (0,)), ((), ()))
NT = (((1,), (1,)), ((), ()))
TN = (((0,), (0,)), ((), ()))


def dotb(a, b, dims=NN):
    return lax.dot_general(a.astype(bf16), b.astype(bf16), dims, preferred_element_type=f32)


def split(a):
    high = a.astype(bf16)
    return high, (a - high.astype(f32)).astype(bf16)


def dot3(a, b, dims=NN):
    ah, al = split(a)
    bh, bl = split(b)
    return dotb(ah, bh, dims) + (dotb(ah, bl, dims) + dotb(al, bh, dims))


def dot_left2(a, b, dims=NN):
    ah, al = split(a)
    return dotb(ah, b, dims) + dotb(al, b, dims)


def sigmoid(x):
    return 1.0 / (1.0 + jnp.exp(-x))


def iota(shape, dim):
    return lax.broadcasted_iota(jnp.int32, shape, dim)


def column(row):
    n = row.shape[1]
    return jnp.sum(jnp.where(iota((n, n), 0) == iota((n, n), 1), row, 0.0), axis=1, keepdims=True)


def chunk_local(r, k, v, dd, cr, doff, coff, extra):
    C = r.shape[1]
    row, col = iota((C, C), 0), iota((C, C), 1)
    u = k * lax.rsqrt(jnp.sum(k * k, axis=0, keepdims=True) + key_eps)
    a = u * sigmoid(cr + coff)
    lg = extra - 0.6065306597126334 * sigmoid(dd + doff)
    lh, lr = split(lg)
    lm, ll = split(lg - lh.astype(f32))
    tri = jnp.where(row <= col, 1.0, 0.0).astype(bf16)
    cum = dotb(lh, tri) + (dotb(lm, tri) + dotb(ll, tri))
    bef = cum - lg
    tot = cum[:, C - 1 : C]
    ref = 0.5 * tot
    en = jnp.exp(ref - cum)
    lhs = jnp.concatenate([u * jnp.exp(bef - ref), r * jnp.exp(cum - ref)], axis=1)
    rhs = jnp.concatenate([k * en, a * en], axis=1)
    G = dotb(lhs, rhs, TN)
    strict, upto = row > col, row >= col
    kp = jnp.where(strict, G[:C, :C], 0.0)
    A = jnp.where(strict, G[:C, C:], 0.0)
    rk = jnp.where(upto, G[C:, :C], 0.0)
    rr = jnp.where(upto, G[C:, C:], 0.0)
    x = row ^ col
    T = jnp.where(row == col, 1.0, 0.0) - jnp.where(x == 1, A, 0.0)
    s = 2
    while s < C:
        m = jnp.where((x >= s) & (x < 2 * s), A, 0.0)
        T = T - dot3(T, dot3(m, T))
        s *= 2
    R = jnp.concatenate([dotb(v, kp, NT), u * jnp.exp(bef)], axis=0)
    X = dotb(R, T, NT)
    out = jnp.concatenate([dotb(v, rk, NT), r * jnp.exp(cum)], axis=0) - dotb(X, rr, NT)
    tail = jnp.exp(tot - cum)
    diag = jnp.where(iota((HD, HD), 0) == iota((HD, HD), 1), jnp.exp(tot), 0.0)
    bm = jnp.concatenate([dotb(v, k * tail, NT), diag], axis=0) - dotb(X, a * tail, NT)
    return out, bm


def whole(
    rT, kT, vT, ddT, crT, gateT, doff, coff, extraT, gain, wmix, xin, fgain, grw, erw, routes,
    wg_hbm, wu_hbm, wd_hbm, wmix_hbm,
    tmo, eo,
    wg, wu, wd, wmp, wload, wsend, wrecv,
    dbuf, X, wch, wcl, dsp_s, dsp_r, ag_s, ag_r,
    outT, qp, xg, xg_s, xg_r, zg, ztot, zg_s, zg_r,
    mx, mxp, mx_s, mx_r, pm, msb, mrb, ms_s, ms_r,
    hid, epm, esb, erb, es_s, es_r, res, home, rt_s, rt_r,
):
    ep, tp = lax.axis_index("ep"), lax.axis_index("tp")
    y, c = tp // 2, tp % 2
    z, x = ep // NX, ep % NX
    half, seat = ep // 16, ep % 16
    partner = (ep, tp + 1 - 2 * c)

    def rdma(src, dst, ssem, rsem, device):
        return pltpu.make_async_remote_copy(
            src_ref=src, dst_ref=dst, send_sem=ssem, recv_sem=rsem, device_id=device, device_id_type=MESH
        )

    def got(ref, sem):
        rdma(ref, ref, sem, sem, partner).wait_recv()

    def sent(ref, sem):
        rdma(ref, ref, sem, sem, partner).wait_send()

    barrier = pltpu.get_barrier_semaphore()

    def greet(device):
        pl.semaphore_signal(barrier, inc=1, device_id=device, device_id_type=MESH)

    def meet(e, _):
        @pl.when(jnp.logical_not((e == ep) & (half == c)))
        def _():
            greet((e, 2 * y + half))

        there, cc = c * 16 + e // 2, e % 2

        @pl.when(jnp.logical_not((there == ep) & (cc == c)))
        def _():
            greet((there, 2 * y + cc))

        return 0

    lax.fori_loop(0, 32, meet, 0)
    greet(partner)
    for d in (1, NY - 1):
        greet((ep, 2 * ((y + d) % NY) + c))
    for d in range(1, NX):
        greet((z * NX + (x + d) % NX, tp))
    for d in range(1, NZ):
        greet(((z + d) % NZ * NX + x, tp))

    loads, swaps = [], []
    for n, (hbm, dst) in enumerate(((wg_hbm, wg), (wu_hbm, wu))):
        for q in range(2):
            loads.append(pltpu.make_async_copy(hbm.at[q], dst.at[0, :, :, q], wload.at[2 * n + q]))
            swaps.append(rdma(hbm.at[q], dst.at[1, :, :, q], wsend.at[2 * n + q], wrecv.at[2 * n + q], partner))
    loads.append(pltpu.make_async_copy(wd_hbm, wd.at[0], wload.at[4]))
    swaps.append(rdma(wd_hbm, wd.at[1], wsend.at[4], wrecv.at[4], partner))
    swaps.append(rdma(wmix_hbm, wmp, wsend.at[5], wrecv.at[5], partner))
    for copy in loads:
        copy.start()

    xf = xin[...].astype(f32)
    rs = lax.rsqrt(jnp.mean(xf * xf, axis=-1, keepdims=True) + norm_eps)
    r0, r1 = routes[0:1, :], routes[1:2, :]
    experts = iota((32, 128), 0)
    m0 = jnp.where(r0 == experts, 1.0, 0.0)
    m1 = jnp.where(r1 == experts, 1.0, 0.0)
    before = jnp.where(iota((128, 128), 0) < iota((128, 128), 1), 1.0, 0.0)
    rank = dotb(m0 + m1, before)
    spread = jnp.where(iota((512, 32), 0) // CAP == iota((512, 32), 1), 1.0, 0.0)
    placed = jnp.where(dotb(spread, rank) == (iota((512, 128), 0) % CAP).astype(f32), dotb(spread, m0 + m1), 0.0)
    fours = y % 4
    for q in range(2):
        cols = pl.ds(pl.multiple_of((2 * fours + 8 * q + c) * 128, 128), 128)
        mine = (xin[:, cols].astype(f32) * rs * fgain[:, cols]).astype(bf16)
        dbuf[:, q * 128 : (q + 1) * 128] = dotb(placed, mine).astype(bf16)

    def dispatch(e, _):
        src = dbuf.at[pl.ds(pl.multiple_of(e * CAP, CAP), CAP), :]
        dst = X.at[
            pl.ds(pl.multiple_of(seat * CAP, CAP), CAP), pl.ds(pl.multiple_of(fours * 512 + c * 256, 128), 256)
        ]
        here = (e == ep) & (half == c)

        @pl.when(here)
        def _():
            pltpu.make_async_copy(src, dst, dsp_r).start()

        @pl.when(jnp.logical_not(here))
        def _():
            rdma(src, dst, dsp_s, dsp_r, (e, 2 * y + half)).start()

        return 0

    def length(d, h):
        return 4 if d == h % 2 else 3

    def at_y(v):
        return (v + 2 * NY) % NY

    def neighbour(d):
        return (ep, 2 * at_y(y + 1 - 2 * d) + c)

    def lanes(s):
        return pl.ds(pl.multiple_of(s * 256, 256), 256)

    def ag_block(place, h):
        return X.at[h * ROWS : (h + 1) * ROWS, pl.ds(pl.multiple_of(at_y(place) % 4 * 512, 512), 512)]

    def behind(d):
        return y - 1 if d == 0 else y + 1

    def ag_copy(d, h, s):
        ref = ag_block(y if s == 0 else behind(d), h)
        return rdma(ref, ref, ag_s.at[d, h, s], ag_r.at[d, h, s], neighbour(d))

    def ag_first():
        for h in range(HALF):
            for d in (h % 2, 1 - h % 2):
                ag_copy(d, h, 0).start()

    def ag_second():
        for h in range(HALF):
            for d in (h % 2, 1 - h % 2):
                got(ag_block(behind(d), h), ag_r.at[d, h, 0])
                if h % 2 == d:
                    ag_copy(d, h, 1).start()

    def ag_done():
        for h in range(HALF):
            got(ag_block(y + 2, h), ag_r.at[h % 2, h, 1])

    def local_chunk(n):
        sl = slice(n * CH, (n + 1) * CH)
        out, bm = chunk_local(
            rT[:, sl].astype(f32), kT[:, sl].astype(f32), vT[:, sl].astype(f32), ddT[:, sl].astype(f32),
            crT[:, sl].astype(f32), column(doff[...]), column(coff[...]), extraT[:, sl],
        )
        outT[n] = out
        return bm

    upper = iota((2 * HD, HD), 0)
    across = iota((2 * HD, HD), 1)

    def join(stack, later_q, later_p):
        return dot_left2(stack, later_p) + jnp.concatenate([later_q, jnp.zeros((HD, HD), f32)], axis=0)

    def rs_step(s, part, sbuf, rbuf, ssem, rsem):
        for h in range(HALF):
            for d in range(2):
                n = length(d, h)
                if s >= n:
                    continue
                dest = at_y(y + (n - s) if d == 0 else y - (n - s))
                value = part(dest, h)
                if s > 0:
                    got(rbuf.at[d, h, s - 1], rsem.at[d, h, s - 1])
                    value = value + rbuf[d, h, s - 1].astype(f32)
                sbuf[d, h, s] = value.astype(bf16)
                rdma(sbuf.at[d, h, s], rbuf.at[d, h, s], ssem.at[d, h, s], rsem.at[d, h, s], neighbour(d)).start()

    def rs_last(h, part, rbuf, rsem):
        value = part(y, h)
        for d in range(2):
            n = length(d, h) - 1
            got(rbuf.at[d, h, n], rsem.at[d, h, n])
            value = value + rbuf[d, h, n].astype(f32)
        return value

    def mix_part(dest, h):
        return pm[dest, :, h * (2048 // HALF) : (h + 1) * (2048 // HALF)]

    @pl.when(half == c)
    def _():
        pl.semaphore_wait(barrier, 62 + 3 + NX - 1 + NZ - 1)

    @pl.when(half != c)
    def _():
        pl.semaphore_wait(barrier, 64 + 3 + NX - 1 + NZ - 1)

    lax.fori_loop(0, 32, dispatch, 0)
    for copy in swaps:
        copy.start()

    bms = [local_chunk(n) for n in range(2)]
    got(X.at[:, pl.ds(pl.multiple_of(fours * 512, 512), 512)], dsp_r)
    ag_first()
    bms += [local_chunk(n) for n in range(2, 4)]
    stack = jnp.where(upper == across + HD, 1.0, 0.0)
    for n in range(4):
        qp[n] = stack
        stack = dot3(stack, bms[n][HD:]) + jnp.where(upper < HD, bms[n], 0.0)
    xg[0] = jnp.concatenate([stack[:HD], stack[HD:]], axis=1).astype(bf16)
    x_copies = []
    for rr in range(1, NX):
        to = (z * NX + (x + rr) % NX, tp)
        x_copies.append(rdma(xg.at[0], xg.at[rr], xg_s.at[rr], xg_r.at[rr], to))
        x_copies[-1].start()

    ag_second()
    for rr in range(1, NX):
        got(xg.at[rr], xg_r.at[rr])
    stack = jnp.where(upper == across + HD, 1.0, 0.0)
    own_q, own_p = jnp.zeros((HD, HD), f32), jnp.zeros((HD, HD), f32)
    for i in range(NX):
        own_q = jnp.where(x == i, stack[:HD], own_q)
        own_p = jnp.where(x == i, stack[HD:], own_p)
        piece = xg[(x - i + NX) % NX].astype(f32)
        stack = join(stack, piece[:, :HD], piece[:, HD:])
    ztot[...] = jnp.concatenate([stack[:HD], stack[HD:]], axis=1).astype(bf16)
    for rr in range(1, NZ):

        @pl.when(z + rr < NZ)
        def _():
            rdma(ztot, zg.at[z], zg_s.at[rr], zg_r.at[z], ((z + rr) * NX + x, tp)).start()

    nb = (xf * rs * fgain[...]).astype(bf16)
    logit = dotb(erw[...], nb, NT)
    gexp = jnp.exp(dotb(grw[...], nb, NT))
    gprob = gexp / jnp.sum(gexp, axis=0, keepdims=True)
    c0 = jnp.sum(jnp.where(r0 == experts, logit, 0.0), axis=0, keepdims=True)
    c1 = jnp.sum(jnp.where(r1 == experts, logit, 0.0), axis=0, keepdims=True)
    groups = iota((GROUPS, 128), 0)
    g0 = jnp.sum(jnp.where(r0 // 8 == groups, gprob, 0.0), axis=0, keepdims=True)
    g1 = jnp.sum(jnp.where(r1 // 8 == groups, gprob, 0.0), axis=0, keepdims=True)
    weight = m0 * (g0 * sigmoid(c0 - c1)) + m1 * (g1 * sigmoid(c1 - c0))
    wh, wl = split(weight)
    full = placed * (dotb(spread, wh) + dotb(spread, wl))
    fh, fl = split(full.T)
    wch[...] = fh
    wcl[...] = fl

    ag_done()
    for copy in loads:
        copy.wait()
    for copy in swaps[:5]:
        copy.wait_recv()
    for q in range(2):
        g = dotb(X[...], wg[q].reshape(2048, 256))
        u = dotb(X[...], wu[q].reshape(2048, 256))
        hid[:, q * 256 : (q + 1) * 256] = (g * sigmoid(g) * u).astype(bf16)

    def down(shift):
        dest = at_y(y + shift)
        epm[dest] = dotb(hid[:, :256], wd[0, :, lanes(dest)]) + dotb(hid[:, 256:], wd[1, :, lanes(dest)])

    def exp_part(dest, h):
        return epm[dest, h * ROWS : (h + 1) * ROWS]

    for shift in (4, 3, -3):
        down(shift)
    rs_step(0, exp_part, esb, erb, es_s, es_r)
    def fold(i, state):
        got(zg.at[i], zg_r.at[i])
        piece = zg[i].astype(f32)
        return dot_left2(state, piece[:, HD:]) + piece[:, :HD]

    state = lax.fori_loop(0, z, fold, jnp.zeros((HD, HD), f32))
    state = dot3(state, own_p) + own_q
    gain_c = column(gain[...])
    for n in range(4):
        sl = slice(n * CH, (n + 1) * CH)
        q = qp[n]
        now = dot3(state, q[HD:]) + q[:HD]
        o = outT[n]
        ho = o[:HD] + dotb(now, o[HD:])
        ho = ho - jnp.mean(ho, axis=0, keepdims=True)
        sp = jnp.mean(ho * ho, axis=0, keepdims=True)
        mixed = ho * lax.rsqrt(sp + group_eps) * gain_c * sigmoid(gateT[:, sl].astype(f32))
        mx[2 * n : 2 * n + 2] = mixed.T.reshape(2, 2, 32, HD).astype(bf16)
    pair = rdma(mx.at[:, 1 - c], mxp, mx_s, mx_r, partner)
    pair.start()
    for shift in (2, -2):
        down(shift)
    rs_step(1, exp_part, esb, erb, es_s, es_r)
    pair.wait_recv()
    swaps[5].wait_recv()
    total = dotb(mx[:, c].reshape(256, HD), wmix[...]) + dotb(mxp[...].reshape(256, HD), wmp[...])
    pm[...] = total.reshape(NY, 32, 2048)

    rs_step(0, mix_part, msb, mrb, ms_s, ms_r)
    for shift in (1, -1, 0):
        down(shift)
    rs_step(2, exp_part, esb, erb, es_s, es_r)
    rs_step(1, mix_part, msb, mrb, ms_s, ms_r)
    rs_step(3, exp_part, esb, erb, es_s, es_r)
    def send_home(n, _):
        j, cc = n // 2, n % 2
        src = res.at[pl.ds(pl.multiple_of(j * CAP, CAP), CAP), pl.ds(pl.multiple_of(cc * 128, 128), 128)]
        dst = home.at[pl.ds(pl.multiple_of(ep * CAP, CAP), CAP), :]
        there = c * 16 + j
        here = (there == ep) & (cc == c)

        @pl.when(here)
        def _():
            pltpu.make_async_copy(src, dst, rt_r).start()

        @pl.when(jnp.logical_not(here))
        def _():
            rdma(src, dst, rt_s, rt_r, (there, 2 * y + cc)).start()

        return 0

    for h in range(HALF):
        res[h * ROWS : (h + 1) * ROWS] = rs_last(h, exp_part, erb, es_r).astype(bf16)
        lax.fori_loop(h * (32 // HALF), (h + 1) * (32 // HALF), send_home, 0)

    rs_step(2, mix_part, msb, mrb, ms_s, ms_r)
    rs_step(3, mix_part, msb, mrb, ms_s, ms_r)
    for h in range(HALF):
        tmo[:, h * (2048 // HALF) : (h + 1) * (2048 // HALF)] = rs_last(h, mix_part, mrb, ms_r).astype(bf16)
    got(home, rt_r)
    eo[...] = (dotb(wch[...], home[...]) + dotb(wcl[...], home[...])).astype(bf16)

    for copy in swaps:
        copy.wait_send()
    for copy in x_copies:
        copy.wait_send()
    for rr in range(1, NZ):

        @pl.when(z + rr < NZ)
        def _():
            sent(ztot, zg_s.at[rr])

    pair.wait_send()

    @pl.when(half == c)
    def _():
        sent(dbuf.at[0:496], dsp_s)
        sent(home.at[0:496], rt_s)

    @pl.when(half != c)
    def _():
        sent(dbuf, dsp_s)
        sent(home, rt_s)

    for d in range(2):
        for h in range(HALF):
            for s in range(length(d, h)):
                if s == 0 or (s == 1 and h % 2 == d):
                    ag_copy(d, h, s).wait_send()
                sent(msb.at[d, h, s], ms_s.at[d, h, s])
                sent(esb.at[d, h, s], es_s.at[d, h, s])


def local(
    receptance, key_matrix, value_matrix, decay_data_term, correction_rate_data, output_gate_input,
    decay_channel_offset, correction_rate_offset, extra_head_log_decay, head_norm_gain, mixer_output_weight,
    expert_layer_input, feedforward_norm_gain, group_router_weight, expert_router_weight, routes,
    expert_gate_weight, expert_up_weight, expert_down_weight,
):
    V = pltpu.VMEM
    DMA = pltpu.SemaphoreType.DMA
    ring = (2, HALF, 4)
    vm = pl.BlockSpec(memory_space=pltpu.VMEM)
    anyw = pl.BlockSpec(memory_space=pl.ANY)
    return pl.pallas_call(
        whole,
        out_shape=(
            jax.ShapeDtypeStruct((32, 2048), bf16),
            jax.ShapeDtypeStruct((128, 128), bf16),
        ),
        in_specs=[vm] * 16 + [anyw] * 4,
        out_specs=(vm, vm),
        scratch_shapes=[
            V((2, 4, 2, 2, 128, 256), bf16), V((2, 4, 2, 2, 128, 256), bf16), V((2, 256, 2048), bf16), V((HD, 2048), bf16),
            DMA((5,)), DMA((6,)), DMA((6,)),
            V((512, 256), bf16), V((256, 2048), bf16), V((128, 512), bf16), V((128, 512), bf16), DMA, DMA, DMA(ring), DMA(ring),
            V((4, 2 * HD, CH), f32), V((4, 2 * HD, HD), f32), V((NX, HD, 2 * HD), bf16), DMA((NX,)), DMA((NX,)),
            V((NZ, HD, 2 * HD), bf16), V((HD, 2 * HD), bf16), DMA((NZ,)), DMA((NZ,)),
            V((NY, 2, 32, HD), bf16), V((NY, 32, HD), bf16), DMA, DMA, V((NY, 32, 2048), f32),
            V((*ring, 32, 2048 // HALF), bf16), V((*ring, 32, 2048 // HALF), bf16), DMA(ring), DMA(ring),
            V((256, 512), bf16), V((NY, 256, 256), f32), V((*ring, ROWS, 256), bf16), V((*ring, ROWS, 256), bf16), DMA(ring), DMA(ring),
            V((256, 256), bf16), V((512, 128), bf16), DMA, DMA,
        ],
        compiler_params=pltpu.CompilerParams(has_side_effects=True, collective_id=0, vmem_limit_bytes=60000 * 1024),
    )(
        receptance.T, key_matrix.T, value_matrix.T, decay_data_term.T, correction_rate_data.T, output_gate_input.T,
        decay_channel_offset.reshape(1, HD), correction_rate_offset.reshape(1, HD), extra_head_log_decay.T,
        head_norm_gain.reshape(1, HD), mixer_output_weight, expert_layer_input, feedforward_norm_gain.reshape(1, 2048),
        group_router_weight.T, expert_router_weight.T, routes.T,
        expert_gate_weight.reshape(2, 4, 2, 128, 256), expert_up_weight.reshape(2, 4, 2, 128, 256), expert_down_weight[0], mixer_output_weight,
    )


def solution(mesh):
    in_specs = (
        P("ep", "tp"), P("ep", "tp"), P("ep", "tp"), P("ep", "tp"), P("ep", "tp"), P("ep", "tp"),
        P("tp"), P("tp"), P("ep", "tp"), P("tp"), P("tp", None),
        P("ep", None), P(), P(), P(), P("ep", None),
        P("ep", None, "tp"), P("ep", None, "tp"), P("ep", "tp", None),
    )
    out_specs = (P(("ep", "tp"), None), P("ep", "tp"))
    return jax.shard_map(local, mesh=mesh, in_specs=in_specs, out_specs=out_specs, check_vma=False)
```

time: 416 us -> 70.3 us (0.17); the launches traced: 410 us -> 70.1 us
  other arithmetic: 108 us -> 0 us
  local copies, waits for them, and re-layouts: 108 us -> 2.19 us
  waiting for transfers between devices: 87.5 us -> 0 us
  Pallas kernels: 0 us -> 67.3 us
  matrix products: 62.7 us -> 0 us
  starting transfers between devices: 42.9 us -> 0 us
    all_to_all x5 -> x0, waiting for transfers between devices: 87.5 us -> none  [the longest x2 77.3 us: summed_on_arrival(): lax.all_to_all(parts, axis, split_axis=0, concat_axis=0, tiled=True)]
    pallas_call x0 -> x1, Pallas kernels: none -> 67.3 us  [local(): pl.pallas_call(whole, out_shape=(jax.ShapeDtypeStruct((32, 2048), bf16),...]
    while x19 -> x0, local copies, waits for them, and re-layouts: 62.4 us -> none
    dot_general x71 -> x0, matrix products: 60.7 us -> none  [the longest x8 7.72 us: block_advance(): jnp.einsum('ihr,ihk->hrk', value_padded, key_b * tail)]
    all_to_all x5 -> x0, starting transfers between devices: 42.9 us -> none  [the longest x2 15.4 us: summed_on_arrival(): lax.all_to_all(parts, axis, split_axis=0, concat_axis=0, tiled=True)]
    another operation x35 -> x0, other arithmetic: 41.1 us -> none  [the longest x24 39.9 us: block_advance(): jax.scipy.linalg.solve_triangular(left_side, right_side, lower=True, unit...]
    select_n x10 -> x0, other arithmetic: 26.8 us -> none  [the longest x8 24.7 us: pair_decay(): return jnp.where(mask, jnp.exp(jnp.where(mask, gap, 0.0)), 0.0)]
    while x8 -> x0, other arithmetic: 25.8 us -> none
  transfers between devices with their start and end apart: 5 -> 0, of which waited for: 4 -> 0; matrix products, arithmetic and copies ran while one was open for 65% -> 0% of each run, Pallas kernels for 0% -> 0%
where the time goes in v2:
time: 70.3 us; the launch traced here: 70.1 us
  Pallas kernels  67.3 us (96%)
  local copies, waits for them, and re-layouts  2.19 us (3%)
    pallas_call x1, Pallas kernels, local(): pl.pallas_call(whole, out_shape=(jax.ShapeDtypeStruct((32, 2048), bf16),...  67.3 us
    unnamed x4, local copies, waits for them, and re-layouts  2.19 us

profile of v2, /device:TPU:1, one launch (start us, length us, event | category | flops | bytes accessed | tf_op | source)
XLA Modules:
  0.0 70.1 jit_solution(12268175975861567322)
XLA Ops:
  0.6 67.3 %shard_map.194 = (bf16[32,2048]{1,0:T(8,128)(2,1)}, bf16[128,128]{1,0:T(8,128)(2,1)}) custom-call(bf16[64,512]{1,0:T(8,128)(2,1)} %bitcast.21, bf16[64,512]{1,0:T(8,128)(2,1)} %bitcast.22, bf16[64,512]{1,0:T(8,128)(2,1)} %bitcast.23, bf16[64,512]{1,0:T(8,128)(2,1)} %bitcast.24, bf16[64,512]{1,0:T(8,128)(2,1)} %bitcast.25, bf16[64,512]{1,0:T(8,128)(2,1)} %bitcast.26, ...), custom_call_target="tpu_custom_call" | custom-call | tf_op jit(solution)/shard_map/pallas_call | solution.py:458
  67.9 0.0 copy-start
  67.9 1.6 %copy.23 = bf16[32,2048]{1,0:T(8,128)(2,1)} copy(bf16[32,2048]{1,0:T(8,128)(2,1)} %get-tuple-element.4) | data formatting | bytes 262144
  69.5 0.0 copy-done
  69.5 0.6 copy.24
Async XLA Ops:
  67.9 1.6 %copy-start = (bf16[128,128]{1,0:T(8,128)(2,1)S(1)}, bf16[128,128]{1,0:T(8,128)(2,1)}, u32[]{:S(2)}) copy-start(bf16[128,128]{1,0:T(8,128)(2,1)} %get-tuple-element.5) | copy-start | bytes 98308

commit v3 on v2

--- a/solution.py
+++ b/solution.py
@@ -57,7 +57,7 @@
     return jnp.sum(jnp.where(iota((n, n), 0) == iota((n, n), 1), row, 0.0), axis=1, keepdims=True)
 
 
-def chunk_local(r, k, v, dd, cr, doff, coff, extra):
+def chunk_pairs(r, k, v, dd, cr, doff, coff, extra):
     C = r.shape[1]
     row, col = iota((C, C), 0), iota((C, C), 1)
     u = k * lax.rsqrt(jnp.sum(k * k, axis=0, keepdims=True) + key_eps)
@@ -79,20 +79,30 @@
     A = jnp.where(strict, G[:C, C:], 0.0)
     rk = jnp.where(upto, G[C:, :C], 0.0)
     rr = jnp.where(upto, G[C:, C:], 0.0)
-    x = row ^ col
-    T = jnp.where(row == col, 1.0, 0.0) - jnp.where(x == 1, A, 0.0)
+    R = jnp.concatenate([dotb(v, kp, NT), u * jnp.exp(bef)], axis=0)
+    out = jnp.concatenate([dotb(v, rk, NT), r * jnp.exp(cum)], axis=0)
+    tail = jnp.exp(tot - cum)
+    diag = jnp.where(iota((HD, HD), 0) == iota((HD, HD), 1), jnp.exp(tot), 0.0)
+    bm = jnp.concatenate([dotb(v, k * tail, NT), diag], axis=0)
+    return A, R, out, rr, bm, a * tail
+
+
+def inverses(pairs):
+    C = pairs[0].shape[0]
+    x = iota((C, C), 0) ^ iota((C, C), 1)
+    found = [jnp.where(x == 0, 1.0, 0.0) - jnp.where(x == 1, A, 0.0) for A in pairs]
     s = 2
     while s < C:
-        m = jnp.where((x >= s) & (x < 2 * s), A, 0.0)
-        T = T - dot3(T, dot3(m, T))
+        level = (x >= s) & (x < 2 * s)
+        right = [dot3(jnp.where(level, A, 0.0), T) for A, T in zip(pairs, found)]
+        found = [T - dot3(T, m) for T, m in zip(found, right)]
         s *= 2
-    R = jnp.concatenate([dotb(v, kp, NT), u * jnp.exp(bef)], axis=0)
+    return found
+
+
+def chunk_ends(T, R, out, rr, bm, at):
     X = dotb(R, T, NT)
-    out = jnp.concatenate([dotb(v, rk, NT), r * jnp.exp(cum)], axis=0) - dotb(X, rr, NT)
-    tail = jnp.exp(tot - cum)
-    diag = jnp.where(iota((HD, HD), 0) == iota((HD, HD), 1), jnp.exp(tot), 0.0)
-    bm = jnp.concatenate([dotb(v, k * tail, NT), diag], axis=0) - dotb(X, a * tail, NT)
-    return out, bm
+    return out - dotb(X, rr, NT), bm - dotb(X, at, NT)
 
 
 def whole(
@@ -231,14 +241,21 @@
         for h in range(HALF):
             got(ag_block(y + 2, h), ag_r.at[h % 2, h, 1])
 
-    def local_chunk(n):
-        sl = slice(n * CH, (n + 1) * CH)
-        out, bm = chunk_local(
-            rT[:, sl].astype(f32), kT[:, sl].astype(f32), vT[:, sl].astype(f32), ddT[:, sl].astype(f32),
-            crT[:, sl].astype(f32), column(doff[...]), column(coff[...]), extraT[:, sl],
-        )
-        outT[n] = out
-        return bm
+    def local_chunks(numbers):
+        pairs = []
+        for n in numbers:
+            sl = slice(n * CH, (n + 1) * CH)
+            pairs.append(
+                chunk_pairs(
+                    rT[:, sl].astype(f32), kT[:, sl].astype(f32), vT[:, sl].astype(f32), ddT[:, sl].astype(f32),
+                    crT[:, sl].astype(f32), column(doff[...]), column(coff[...]), extraT[:, sl],
+                )
+            )
+        bms = []
+        for n, T, p in zip(numbers, inverses([p[0] for p in pairs]), pairs):
+            outT[n], bm = chunk_ends(T, *p[1:])
+            bms.append(bm)
+        return bms
 
     upper = iota((2 * HD, HD), 0)
     across = iota((2 * HD, HD), 1)
@@ -283,10 +300,7 @@
     for copy in swaps:
         copy.start()
 
-    bms = [local_chunk(n) for n in range(2)]
-    got(X.at[:, pl.ds(pl.multiple_of(fours * 512, 512), 512)], dsp_r)
-    ag_first()
-    bms += [local_chunk(n) for n in range(2, 4)]
+    bms = local_chunks((0, 1, 2, 3))
     stack = jnp.where(upper == across + HD, 1.0, 0.0)
     for n in range(4):
         qp[n] = stack
@@ -298,7 +312,8 @@
         x_copies.append(rdma(xg.at[0], xg.at[rr], xg_s.at[rr], xg_r.at[rr], to))
         x_copies[-1].start()
 
-    ag_second()
+    got(X.at[:, pl.ds(pl.multiple_of(fours * 512, 512), 512)], dsp_r)
+    ag_first()
     for rr in range(1, NX):
         got(xg.at[rr], xg_r.at[rr])
     stack = jnp.where(upper == across + HD, 1.0, 0.0)
@@ -315,6 +330,7 @@
         def _():
             rdma(ztot, zg.at[z], zg_s.at[rr], zg_r.at[z], ((z + rr) * NX + x, tp)).start()
 
+    ag_second()
     nb = (xf * rs * fgain[...]).astype(bf16)
     logit = dotb(erw[...], nb, NT)
     gexp = jnp.exp(dotb(grw[...], nb, NT))

time: 70.3 us -> 68.6 us (0.976)
  Pallas kernels: 67.3 us -> 65.6 us
    pallas_call x1, Pallas kernels: 67.3 us -> 65.6 us  [local(): pl.pallas_call(whole, out_shape=(jax.ShapeDtypeStruct((32, 2048), bf16),...]
where the time goes in v3:
time: 68.6 us; the launch traced here: 68.5 us
  Pallas kernels  65.6 us (96%)
  local copies, waits for them, and re-layouts  2.19 us (3%)
    pallas_call x1, Pallas kernels, local(): pl.pallas_call(whole, out_shape=(jax.ShapeDtypeStruct((32, 2048), bf16),...  65.6 us
    unnamed x4, local copies, waits for them, and re-layouts  2.19 us

profile of v3, /device:TPU:1, one launch (start us, length us, event | category | flops | bytes accessed | tf_op | source)
XLA Modules:
  0.0 68.5 jit_solution(3816113869651276339)
XLA Ops:
  0.6 65.6 %shard_map.194 = (bf16[32,2048]{1,0:T(8,128)(2,1)}, bf16[128,128]{1,0:T(8,128)(2,1)}) custom-call(bf16[64,512]{1,0:T(8,128)(2,1)} %bitcast.21, bf16[64,512]{1,0:T(8,128)(2,1)} %bitcast.22, bf16[64,512]{1,0:T(8,128)(2,1)} %bitcast.23, bf16[64,512]{1,0:T(8,128)(2,1)} %bitcast.24, bf16[64,512]{1,0:T(8,128)(2,1)} %bitcast.25, bf16[64,512]{1,0:T(8,128)(2,1)} %bitcast.26, ...), custom_call_target="tpu_custom_call" | custom-call | tf_op jit(solution)/shard_map/pallas_call | solution.py:474
  66.3 0.0 copy-start
  66.3 1.6 %copy.23 = bf16[32,2048]{1,0:T(8,128)(2,1)} copy(bf16[32,2048]{1,0:T(8,128)(2,1)} %get-tuple-element.4) | data formatting | bytes 262144
  67.9 0.0 copy-done
  67.9 0.6 copy.24
Async XLA Ops:
  66.3 1.6 %copy-start = (bf16[128,128]{1,0:T(8,128)(2,1)S(1)}, bf16[128,128]{1,0:T(8,128)(2,1)}, u32[]{:S(2)}) copy-start(bf16[128,128]{1,0:T(8,128)(2,1)} %get-tuple-element.5) | copy-start | bytes 98308

commit v4 on v3

--- a/solution.py
+++ b/solution.py
@@ -424,11 +424,11 @@
 
     rs_step(2, mix_part, msb, mrb, ms_s, ms_r)
     rs_step(3, mix_part, msb, mrb, ms_s, ms_r)
+    got(home, rt_r)
+    eo[...] = (dotb(wch[...], home[...]) + dotb(wcl[...], home[...])).astype(bf16)
+
     for h in range(HALF):
         tmo[:, h * (2048 // HALF) : (h + 1) * (2048 // HALF)] = rs_last(h, mix_part, mrb, ms_r).astype(bf16)
-    got(home, rt_r)
-    eo[...] = (dotb(wch[...], home[...]) + dotb(wcl[...], home[...])).astype(bf16)
-
     for copy in swaps:
         copy.wait_send()
     for copy in x_copies:

time: 68.6 us -> 68.7 us (level)
  no operation moved by 1% of the time
where the time goes in v4:
time: 68.7 us; the launch traced here: 68.6 us
  Pallas kernels  65.7 us (96%)
  local copies, waits for them, and re-layouts  2.19 us (3%)
    pallas_call x1, Pallas kernels, local(): pl.pallas_call(whole, out_shape=(jax.ShapeDtypeStruct((32, 2048), bf16),...  65.7 us
    unnamed x4, local copies, waits for them, and re-layouts  2.19 us

profile of v4, /device:TPU:1, one launch (start us, length us, event | category | flops | bytes accessed | tf_op | source)
XLA Modules:
  0.0 68.6 jit_solution(11006728065328612948)
XLA Ops:
  0.6 65.7 %shard_map.194 = (bf16[32,2048]{1,0:T(8,128)(2,1)}, bf16[128,128]{1,0:T(8,128)(2,1)}) custom-call(bf16[64,512]{1,0:T(8,128)(2,1)} %bitcast.21, bf16[64,512]{1,0:T(8,128)(2,1)} %bitcast.22, bf16[64,512]{1,0:T(8,128)(2,1)} %bitcast.23, bf16[64,512]{1,0:T(8,128)(2,1)} %bitcast.24, bf16[64,512]{1,0:T(8,128)(2,1)} %bitcast.25, bf16[64,512]{1,0:T(8,128)(2,1)} %bitcast.26, ...), custom_call_target="tpu_custom_call" | custom-call | tf_op jit(solution)/shard_map/pallas_call | solution.py:474
  66.4 0.0 copy-start
  66.4 1.6 %copy.23 = bf16[32,2048]{1,0:T(8,128)(2,1)} copy(bf16[32,2048]{1,0:T(8,128)(2,1)} %get-tuple-element.4) | data formatting | bytes 262144
  67.9 0.0 copy-done
  67.9 0.6 copy.24
Async XLA Ops:
  66.4 1.6 %copy-start = (bf16[128,128]{1,0:T(8,128)(2,1)S(1)}, bf16[128,128]{1,0:T(8,128)(2,1)}, u32[]{:S(2)}) copy-start(bf16[128,128]{1,0:T(8,128)(2,1)} %get-tuple-element.5) | copy-start | bytes 98308
